TPU v7x, 128 devices: a whole 4x4x4 slice. The times are simulated.
128 devices in a mesh: ep: 128 (over z, y, x, core).
Axes of the slice: x: 4, y: 4, z: 4, core: 2. Of those that a mesh axis runs over, the one named last changes fastest.
Arguments:
- residual_in: bfloat16 [1024, 2048], P('ep'), may hold values from -6 to 6
- gain_mix_pre: float32 [2048], replicated, may hold values from 0.1 to 1.9
- w_query: bfloat16 [2048, 2048], P(None, 'ep'), may hold values from -0.125 to 0.125
- w_key: bfloat16 [2048, 2048], P(None, 'ep'), may hold values from -0.125 to 0.125
- w_value: bfloat16 [2048, 2048], P(None, 'ep'), may hold values from -0.125 to 0.125
- w_outgate: bfloat16 [2048, 2048], P(None, 'ep'), may hold values from -0.125 to 0.125
- w_decay: bfloat16 [2048, 16], replicated, may hold values from -0.125 to 0.125
- w_beta: bfloat16 [2048, 16], replicated, may hold values from -0.125 to 0.125
- decay_scale: float32 [16], replicated, may hold values from 1 to 16
- decay_bias: float32 [16], replicated, may hold values from -5 to -1
- head_gain: float32 [128], replicated, may hold values from 0.1 to 1.9
- w_out: bfloat16 [2048, 2048], replicated, may hold values from -0.125 to 0.125
- gain_mix_post: float32 [2048], replicated, may hold values from 0.1 to 1.9
- state_cache: bfloat16 [1024, 16, 128, 128], P('ep'), may hold values from -2.390625 to 2.390625
- gain_ffn_pre: float32 [2048], replicated, may hold values from 0.1 to 1.9
- routes: int32 [1024, 4], P('ep'), may hold values from 0 to 31, all different within a row; in each aligned block of 8 rows (0 to 7, 8 to 15, ...) at most 2 rows name the same one
- route_logits: float32 [1024, 4], P('ep'), may hold values from -6 to 6
- w_gate: bfloat16 [2048, 65536], P(None, 'ep'), may hold values from -0.375 to 0.375
- w_up: bfloat16 [2048, 65536], P(None, 'ep'), may hold values from -0.375 to 0.375
- w_down: bfloat16 [65536, 2048], P('ep'), may hold values from -0.125 to 0.125
- gain_ffn_post: float32 [2048], replicated, may hold values from 0.1 to 1.9
Outputs:
- result: bfloat16 [1024, 2048], P('ep')
- new_state: bfloat16 [1024, 16, 128, 128], P('ep')
Inputs may be any that keep to these rules, and one draw needn't show every extreme that they name: `routes`: each row names 4 different experts. In the rows of one device (aligned blocks of 8 rows) no expert is named more than 2 times, and in some block one expert is named exactly 2 times.
All inputs are finite; a program needn't handle non-finite values.
Results may differ from a plain program's by a relative error of at most 0.014.
Values may be sent and summed in bfloat16 or wider, within the bound.
No kernel may reach another device: no remote copies, remote signals or barrier semaphores. Data moves between devices by JAX's collectives and lax.ppermute only.
A program may use at most 128 MiB of HBM per device.

v0:
```python
import jax
import jax.numpy as jnp
from jax import lax
from jax.sharding import PartitionSpec as P

H = 16
HD = 128
PIECES = 4
TOPK = 4


EPS = 1e-06
LIMIT = 7.0
ALPHA = 1.702


def rms_scale(values):
    return values * lax.rsqrt(jnp.mean(values * values, axis=-1, keepdims=True) + EPS)


def clamped_unit(gate, upper):
    glu = jnp.minimum(gate, LIMIT)
    linear = jnp.clip(upper, -LIMIT, LIMIT)
    return glu * jax.nn.sigmoid(ALPHA * glu) * (linear + 1.0)


def dispatch_table(routes, experts, capacity):
    count, topk = routes.shape
    hits = (routes[:, :, None] == jnp.arange(experts, dtype=jnp.int32)).astype(jnp.int32)
    flat = hits.reshape(count * topk, experts)
    before = jnp.cumsum(flat, axis=0) - flat
    slots = jnp.sum(before * flat, axis=1).reshape(count, topk)
    target = routes * capacity + slots
    return (target[:, :, None] == jnp.arange(experts * capacity, dtype=jnp.int32)).astype(
        jnp.float32
    )


def delta_step(
    q_raw, k_raw, v_raw, z_raw, decay_in, beta_in, state, decay_scale, decay_bias, head_gain
):
    count = q_raw.shape[0]
    query = jax.nn.silu(q_raw.astype(jnp.float32)).reshape(count, H, HD)
    query = query * lax.rsqrt(jnp.sum(query * query, axis=-1, keepdims=True) + EPS) * HD ** (-0.5)
    keys = jax.nn.silu(k_raw.astype(jnp.float32)).reshape(count, H, HD)
    keys = keys * lax.rsqrt(jnp.sum(keys * keys, axis=-1, keepdims=True) + EPS)
    values = jax.nn.silu(v_raw.astype(jnp.float32)).reshape(count, H, HD)
    decay = -decay_scale * jax.nn.softplus(decay_in + decay_bias)
    beta = jax.nn.sigmoid(beta_in)
    held = state.astype(jnp.float32) * jnp.exp(decay)[:, :, None, None]
    guess = jnp.einsum("rhk,rhkv->rhv", keys, held)
    held = held + jnp.einsum("rhk,rhv->rhkv", keys, beta[:, :, None] * (values - guess))
    output = jnp.einsum("rhk,rhkv->rhv", query, held)
    output = rms_scale(output) * head_gain
    gated = output.reshape(count, H * HD) * jax.nn.silu(z_raw.astype(jnp.float32))
    return (gated.astype(jnp.bfloat16), held.astype(jnp.bfloat16))


def shards(
    residual_in,
    gain_mix_pre,
    w_query,
    w_key,
    w_value,
    w_outgate,
    w_decay,
    w_beta,
    decay_scale,
    decay_bias,
    head_gain,
    w_out,
    gain_mix_post,
    state_cache,
    gain_ffn_pre,
    routes,
    route_logits,
    w_gate,
    w_up,
    w_down,
    gain_ffn_post,
):
    devices = lax.axis_size("ep")
    count, width = residual_in.shape
    x_first = residual_in.astype(jnp.float32)
    normed = (rms_scale(x_first) * gain_mix_pre).astype(jnp.bfloat16)
    stacked = jnp.stack([w_query, w_key, w_value, w_outgate])
    columns = jnp.einsum(
        "td,rdc->trc",
        lax.all_gather(normed, "ep", axis=0, tiled=True),
        stacked,
        preferred_element_type=jnp.float32,
    ).astype(jnp.bfloat16)
    joined = lax.all_to_all(columns, "ep", split_axis=0, concat_axis=2, tiled=True)
    decay_in = jnp.dot(normed, w_decay, preferred_element_type=jnp.float32)
    beta_in = jnp.dot(normed, w_beta, preferred_element_type=jnp.float32)
    mixed, new_state = delta_step(
        joined[:, 0],
        joined[:, 1],
        joined[:, 2],
        joined[:, 3],
        decay_in,
        beta_in,
        state_cache,
        decay_scale,
        decay_bias,
        head_gain,
    )
    branch = jnp.dot(mixed, w_out, preferred_element_type=jnp.float32)
    x_second = x_first + rms_scale(branch) * gain_mix_post
    normed_two = (rms_scale(x_second) * gain_ffn_pre).astype(jnp.bfloat16)
    experts = devices // PIECES
    capacity = max(2, 2 * count * TOPK // experts)
    table = dispatch_table(routes, experts, capacity)
    picks = jnp.sum(table, axis=1).astype(jnp.bfloat16)
    sent = lax.dot_general(
        picks, normed_two, (((0,), (0,)), ((), ())), preferred_element_type=jnp.float32
    ).astype(jnp.bfloat16)
    sent = jnp.broadcast_to(
        sent.reshape(experts, 1, capacity, width), (experts, PIECES, capacity, width)
    ).reshape(devices, capacity, width)
    block = lax.all_to_all(sent, "ep", split_axis=0, concat_axis=0, tiled=True)
    flat = block.reshape(-1, width)
    hidden = clamped_unit(
        jnp.dot(flat, w_gate, preferred_element_type=jnp.float32),
        jnp.dot(flat, w_up, preferred_element_type=jnp.float32),
    ).astype(jnp.bfloat16)
    partial_value = jnp.dot(hidden, w_down, preferred_element_type=jnp.float32).astype(jnp.bfloat16)
    returned = lax.all_to_all(
        partial_value.reshape(block.shape), "ep", split_axis=0, concat_axis=0, tiled=True
    )
    summed = jnp.sum(returned.reshape(experts, PIECES, capacity, width).astype(jnp.float32), axis=1)
    summed = summed.reshape(experts * capacity, width)
    raised = jnp.exp(route_logits)
    weights = raised / jnp.sum(raised, axis=-1, keepdims=True)
    mix_table = jnp.einsum("ske,sk->se", table, weights)
    moe = jnp.dot(mix_table, summed)
    result = (x_second + rms_scale(moe) * gain_ffn_post).astype(jnp.bfloat16)
    return (result, new_state)


def solution(mesh):
    in_specs = (
        P("ep", None),
        P(),
        P(None, "ep"),
        P(None, "ep"),
        P(None, "ep"),
        P(None, "ep"),
        P(),
        P(),
        P(),
        P(),
        P(),
        P(),
        P(),
        P("ep", None, None, None),
        P(),
        P("ep", None),
        P("ep", None),
        P(None, "ep"),
        P(None, "ep"),
        P("ep", None),
        P(),
    )
    out_specs = (P("ep", None), P("ep", None, None, None))
    return jax.shard_map(shards, mesh=mesh, in_specs=in_specs, out_specs=out_specs, check_vma=False)
```

profile of v0, /device:TPU:0, one launch (start us, length us, event | category | flops | bytes accessed | tf_op | source)
XLA Modules:
  0.0 186.5 jit_solution(18092461676442256661)
XLA Ops:
  7.2 1.0 fusion.38
  8.3 1.5 fusion.40
  11.6 1.0 fusion.12
  12.6 1.0 fusion.57
  14.6 66.2 %all-gather.2.cloned.1.call-done = bf16[1024,2048]{1,0:T(8,128)(2,1)} async-done(((bf16[8,2048]{1,0:T(8,128)(2,1)}), bf16[1024,2048]{1,0:T(8,128)(2,1)}) %all-gather.2.cloned.1.call-update) | async-done | bytes 4194320 | tf_op jit(solution)/shard_map/all_gather | solution.py:89
  80.8 3.6 %fusion.65 = f32[1024,64]{0,1:S(1)} fusion(bf16[1024,2048]{1,0:T(8,128)(2,1)} %all-gather.2.cloned.1.call-done, bf16[2048,64]{0,1:T(8,128)(2,1)S(1)} %bitcast.103), kind=kOutput, calls=%fused_computation.116 | convolution fusion | flops 268435456 | bytes 4718592
  85.1 1.5 reshape.127
  86.6 6.3 %all-to-all-start = ((bf16[128,2,256]{2,1,0:T(2,128)(2,1)}), bf16[128,2,256]{2,1,0:T(2,128)(2,1)S(1)}, u32[]{:S(2)}, u32[]{:S(2)}) async-start(bf16[128,2,256]{2,1,0:T(2,128)(2,1)} %reshape.127), calls=%async_computation | async-start | bytes 262144 | tf_op jit(solution)/shard_map/all_to_all | solution.py:93
  93.2 9.1 %all-to-all-done = bf16[128,2,256]{2,1,0:T(2,128)(2,1)S(1)} async-done(((bf16[128,2,256]{2,1,0:T(2,128)(2,1)}), bf16[128,2,256]{2,1,0:T(2,128)(2,1)S(1)}, u32[]{:S(2)}, u32[]{:S(2)}) %all-to-all-start) | async-done | bytes 131104 | tf_op jit(solution)/shard_map/all_to_all | solution.py:93
  103.4 1.8 all_to_all.22
  105.4 3.6 %fusion = f32[8,16,1,128]{3,2,1,0:T(1,128)S(1)} fusion(bf16[8,16,128,128]{3,2,1,0:T(8,128)(2,1)} %param.34, f32[8,16]{1,0:T(8,128)S(1)} %fusion.57, bf16[8,16,128,1]{2,0,1,3:T(8,128)(2,1)S(1)} %get-tuple-element.5), kind=kOutput, calls=%fused_computation.2 | convolution fusion | flops 8388608 | bytes 4293120 | tf_op jit(solution)/shard_map/rhk,rhkv->rhv/dot_general | solution.py:51
  109.2 3.8 %fusion.2 = f32[8,16,1,128]{3,2,1,0:T(1,128)S(1)} fusion(bf16[8,16,128,128]{3,2,1,0:T(8,128)(2,1)S(1)} %copy-done.1, f32[8,16,128]{2,1,0:T(8,128)S(1)} %copy.46, f32[8,16,128]{2,1,0:T(8,128)S(1)} %copy.44, f32[8,16]{1,0:T(8,128)S(1)} %fusion.57, bf16[8,16,128,1]{2,0,1,3:T(8,128)(2,1)S(1)} %get-tuple-element.4), kind=kOutput, calls=%fused_computation.4 | convolution fusion | flops 12582912 | bytes 4424192 | tf_op jit(solution)/shard_map/rhk,rhkv->rhv/dot_general | solution.py:53
  113.2 4.7 %multiply_reduce_fusion.2 = (f32[8]{0:T(128)S(1)}, f32[8,2048]{1,0:T(8,128)S(1)}) fusion(bf16[2048,2048]{1,0:T(8,128)(2,1)} %param.32, f32[8,16,1,128]{3,2,1,0:T(1,128)S(1)} %fusion.2, bf16[8,4,2048]{2,0,1:T(8,128)(2,1)S(1)} %all_to_all.22, f32[128]{0:T(128)S(1)} %copy-done.7, f32[8,16]{0,1:T(8,128)S(1)} %add_rsqrt_fusion), kind=kOutput, calls=%fused_computation.73 | convolution fusion | flops 67289080 | bytes 8561184 | tf_op jit(solution)/shard_map/dot_general | solution.py:108
  118.7 1.6 broadcast_in_dim.5
  120.3 5.0 %all-to-all-start.1 = ((bf16[128,2,2048]{2,1,0:T(2,128)(2,1)}), bf16[128,2,2048]{2,1,0:T(2,128)(2,1)S(1)}, u32[]{:S(2)}, u32[]{:S(2)}) async-start(bf16[128,2,2048]{2,1,0:T(2,128)(2,1)} %bitcast.25), calls=%async_computation.1 | async-start | bytes 2097152 | tf_op jit(solution)/shard_map/all_to_all | solution.py:121
  125.3 18.9 %all-to-all-done.1 = bf16[128,2,2048]{2,1,0:T(2,128)(2,1)S(1)} async-done(((bf16[128,2,2048]{2,1,0:T(2,128)(2,1)}), bf16[128,2,2048]{2,1,0:T(2,128)(2,1)S(1)}, u32[]{:S(2)}, u32[]{:S(2)}) %all-to-all-start.1) | async-done | bytes 1048608 | tf_op jit(solution)/shard_map/all_to_all | solution.py:121
  144.2 1.2 reshape.111
  145.4 3.4 %convolution_minimum_fusion = f32[256,512]{1,0:T(8,128)} fusion(bf16[256,2048]{1,0:T(8,128)(2,1)} %reshape.111, bf16[2048,512]{1,0:T(8,128)(2,1)} %param.38), kind=kOutput, calls=%fused_computation.13 | convolution fusion | flops 537001984 | bytes 3670016 | tf_op jit(solution)/shard_map/dot_general | solution.py:124
  148.9 3.4 %convolution_convert_fusion = bf16[256,2048]{1,0:T(8,128)(2,1)S(1)} fusion(bf16[512,2048]{1,0:T(8,128)(2,1)S(1)} %copy-done, bf16[256,2048]{1,0:T(8,128)(2,1)} %reshape.111, bf16[2048,512]{1,0:T(8,128)(2,1)} %param.39, f32[256,512]{1,0:T(8,128)} %convolution_minimum_fusion), kind=kOutput, calls=%fused_computation.9 | convolution fusion | flops 1075445760 | bytes 6815744 | tf_op jit(solution)/shard_map/dot_general | solution.py:127
  152.2 1.5 reshape.112
  153.8 4.6 %all-to-all-start.2 = ((bf16[128,2,2048]{2,1,0:T(2,128)(2,1)}), bf16[128,2,2048]{2,1,0:T(2,128)(2,1)S(1)}, u32[]{:S(2)}, u32[]{:S(2)}) async-start(bf16[128,2,2048]{2,1,0:T(2,128)(2,1)} %reshape.112), calls=%async_computation.2 | async-start | bytes 2097152 | tf_op jit(solution)/shard_map/all_to_all | solution.py:128
  158.7 6.0 %fusion.1 = bf16[8,16,128,128]{3,2,1,0:T(8,128)(2,1)} fusion(bf16[8,16,128,128]{3,2,1,0:T(8,128)(2,1)} %param.34, f32[8,16,128]{2,1,0:T(8,128)S(1)} %copy.46, f32[8,16,128]{2,1,0:T(8,128)S(1)} %copy.44, f32[8,16]{1,0:T(8,128)S(1)} %fusion.57), kind=kLoop, calls=%fused_computation.3 | loop fusion | flops 10485760 | bytes 8520192 | tf_op jit(solution)/shard_map/convert_element_type | solution.py:56
  164.7 12.8 %all-to-all-done.2 = bf16[128,2,2048]{2,1,0:T(2,128)(2,1)S(1)} async-done(((bf16[128,2,2048]{2,1,0:T(2,128)(2,1)}), bf16[128,2,2048]{2,1,0:T(2,128)(2,1)S(1)}, u32[]{:S(2)}, u32[]{:S(2)}) %all-to-all-start.2) | async-done | bytes 1048608 | tf_op jit(solution)/shard_map/all_to_all | solution.py:128
  177.5 1.0 convert_reduce_fusion
  (58 shorter events, 7.6 us)
Async XLA Ops:
  7.2 141.7 %copy-start = (bf16[512,2048]{1,0:T(8,128)(2,1)S(1)}, bf16[512,2048]{1,0:T(8,128)(2,1)}, u32[]{:S(2)}) copy-start(bf16[512,2048]{1,0:T(8,128)(2,1)} %param.40) | copy-start | bytes 6291460
  7.2 73.6 %all-gather.2.cloned.1.call-start = ((), (), s32[]{:S(2)}) async-start(), calls=%async_computation.3 | async-start | bytes 4227072 | tf_op jit(solution)/shard_map/all_gather | solution.py:89
  86.6 15.7 %all-to-all-start = ((bf16[128,2,256]{2,1,0:T(2,128)(2,1)}), bf16[128,2,256]{2,1,0:T(2,128)(2,1)S(1)}, u32[]{:S(2)}, u32[]{:S(2)}) async-start(bf16[128,2,256]{2,1,0:T(2,128)(2,1)} %reshape.127), calls=%async_computation | async-start | bytes 262144 | tf_op jit(solution)/shard_map/all_to_all | solution.py:93
  105.2 4.0 %copy-start.1 = (bf16[8,16,128,128]{3,2,1,0:T(8,128)(2,1)S(1)}, bf16[8,16,128,128]{3,2,1,0:T(8,128)(2,1)}, u32[]{:S(2)}) copy-start(bf16[8,16,128,128]{3,2,1,0:T(8,128)(2,1)} %param.34) | copy-start | bytes 12582916
  109.2 3.9 %copy-start.7 = (f32[128]{0:T(128)S(1)}, f32[128]{0:T(128)}, u32[]{:S(2)}) copy-start(f32[128]{0:T(128)} %param.31) | copy-start | bytes 1540
  113.2 4.8 %copy-start.2 = (bf16[8,2048]{1,0:T(8,128)(2,1)S(1)}, bf16[8,2048]{1,0:T(8,128)(2,1)}, u32[]{:S(2)}) copy-start(bf16[8,2048]{1,0:T(8,128)(2,1)} %param.21) | copy-start | bytes 98308
  113.2 4.8 %copy-start.3 = (f32[2048]{0:T(1024)S(1)}, f32[2048]{0:T(1024)}, u32[]{:S(2)}) copy-start(f32[2048]{0:T(1024)} %param.33) | copy-start | bytes 24580
  113.2 5.0 %copy-start.4 = (f32[2048]{0:T(1024)S(1)}, f32[2048]{0:T(1024)}, u32[]{:S(2)}) copy-start(f32[2048]{0:T(1024)} %param.35) | copy-start | bytes 24580
  117.9 7.4 %copy-start.5 = (f32[8,4]{0,1:T(4,128)S(1)}, f32[8,4]{0,1:T(4,128)}, u32[]{:S(2)}) copy-start(f32[8,4]{0,1:T(4,128)} %param.37) | copy-start | bytes 388
  120.3 24.0 %all-to-all-start.1 = ((bf16[128,2,2048]{2,1,0:T(2,128)(2,1)}), bf16[128,2,2048]{2,1,0:T(2,128)(2,1)S(1)}, u32[]{:S(2)}, u32[]{:S(2)}) async-start(bf16[128,2,2048]{2,1,0:T(2,128)(2,1)} %bitcast.25), calls=%async_computation.1 | async-start | bytes 2097152 | tf_op jit(solution)/shard_map/all_to_all | solution.py:121
  153.8 23.8 %all-to-all-start.2 = ((bf16[128,2,2048]{2,1,0:T(2,128)(2,1)}), bf16[128,2,2048]{2,1,0:T(2,128)(2,1)S(1)}, u32[]{:S(2)}, u32[]{:S(2)}) async-start(bf16[128,2,2048]{2,1,0:T(2,128)(2,1)} %reshape.112), calls=%async_computation.2 | async-start | bytes 2097152 | tf_op jit(solution)/shard_map/all_to_all | solution.py:128
  158.7 20.2 %copy-start.6 = (f32[2048]{0:T(1024)S(1)}, f32[2048]{0:T(1024)}, u32[]{:S(2)}) copy-start(f32[2048]{0:T(1024)} %param.41) | copy-start | bytes 24580
Sparse Core Ops, SparseCore 0:
  11.7 69.0 all-gather.1
where the time goes:
time: 188 us; the launch traced here: 186 us
  waiting for transfers between devices  107 us (57%)
  matrix products  25.2 us (13%)
  starting transfers between devices  16 us (9%)
  between operations  14.3 us (8%)
  other arithmetic  13 us (7%)
  local copies, waits for them, and re-layouts  10.9 us (6%)
    all_gather x1, waiting for transfers between devices, shards(): lax.all_gather(normed, 'ep', axis=0, tiled=True)  66.2 us
    all_to_all x1, waiting for transfers between devices, shards(): block = lax.all_to_all(sent, 'ep', split_axis=0, concat_axis=0, tiled=True)  18.9 us
    all_to_all x1, waiting for transfers between devices, shards(): lax.all_to_all(partial_value.reshape(block.shape), 'ep', split_axis=0, co...  12.8 us
    all_to_all x1, waiting for transfers between devices, shards(): lax.all_to_all(columns, 'ep', split_axis=0, concat_axis=2, tiled=True)  9.14 us
    all_to_all x1, starting transfers between devices, shards(): lax.all_to_all(columns, 'ep', split_axis=0, concat_axis=2, tiled=True)  6.29 us
    convert_element_type x1, other arithmetic, delta_step(): return (gated.astype(jnp.bfloat16), held.astype(jnp.bfloat16))  5.96 us
    all_to_all x1, starting transfers between devices, shards(): block = lax.all_to_all(sent, 'ep', split_axis=0, concat_axis=0, tiled=True)  5.01 us
    dot_general x1, matrix products, shards(): branch = jnp.dot(mixed, w_out, preferred_element_type=jnp.float32)  4.73 us
  transfers between devices with their start and end apart: 4, of which 4 were waited for; matrix products, arithmetic and copies ran while one was open for 6% of the time, Pallas kernels for 0%

commit v1 on v0

v1 whole, which is shorter than its diff:
```python
import jax
import jax.numpy as jnp
from jax import lax
from jax.sharding import Mesh
from jax.sharding import PartitionSpec as P

H = 16
HD = 128
TOPK = 4
EXPERTS = 32
CAP = 2
ZY = 16
CHIPS = 64
QUART = 4


EPS = 1e-06
LIMIT = 7.0
ALPHA = 1.702


def rms_scale(values):
    return values * lax.rsqrt(jnp.mean(values * values, axis=-1, keepdims=True) + EPS)


def clamped_unit(gate, upper):
    glu = jnp.minimum(gate, LIMIT)
    linear = jnp.clip(upper, -LIMIT, LIMIT)
    return glu * jax.nn.sigmoid(ALPHA * glu) * (linear + 1.0)


def dispatch_table(routes, experts, capacity):
    count, topk = routes.shape
    hits = (routes[:, :, None] == jnp.arange(experts, dtype=jnp.int32)).astype(jnp.int32)
    flat = hits.reshape(count * topk, experts)
    before = jnp.cumsum(flat, axis=0) - flat
    slots = jnp.sum(before * flat, axis=1).reshape(count, topk)
    target = routes * capacity + slots
    return (target[:, :, None] == jnp.arange(experts * capacity, dtype=jnp.int32)).astype(
        jnp.float32
    )


def delta_step(
    q_raw, k_raw, v_raw, z_raw, decay_in, beta_in, state, decay_scale, decay_bias, head_gain
):
    count = q_raw.shape[0]
    query = jax.nn.silu(q_raw.astype(jnp.float32)).reshape(count, H, HD)
    query = query * lax.rsqrt(jnp.sum(query * query, axis=-1, keepdims=True) + EPS) * HD ** (-0.5)
    keys = jax.nn.silu(k_raw.astype(jnp.float32)).reshape(count, H, HD)
    keys = keys * lax.rsqrt(jnp.sum(keys * keys, axis=-1, keepdims=True) + EPS)
    values = jax.nn.silu(v_raw.astype(jnp.float32)).reshape(count, H, HD)
    decay = -decay_scale * jax.nn.softplus(decay_in + decay_bias)
    beta = jax.nn.sigmoid(beta_in)
    held = state.astype(jnp.float32) * jnp.exp(decay)[:, :, None, None]
    guess = jnp.einsum("rhk,rhkv->rhv", keys, held)
    held = held + jnp.einsum("rhk,rhv->rhkv", keys, beta[:, :, None] * (values - guess))
    output = jnp.einsum("rhk,rhkv->rhv", query, held)
    output = rms_scale(output) * head_gain
    gated = output.reshape(count, H * HD) * jax.nn.silu(z_raw.astype(jnp.float32))
    return (gated.astype(jnp.bfloat16), held.astype(jnp.bfloat16))


def swap_cores(values):
    return lax.ppermute(values, "c", [(0, 1), (1, 0)])


def shards(
    residual_in,
    gain_mix_pre,
    w_query,
    w_key,
    w_value,
    w_outgate,
    w_decay,
    w_beta,
    decay_scale,
    decay_bias,
    head_gain,
    w_out,
    gain_mix_post,
    state_cache,
    gain_ffn_pre,
    routes,
    route_logits,
    w_gate,
    w_up,
    w_down,
    gain_ffn_post,
):
    count, width = residual_in.shape
    x_at = lax.axis_index("x")
    c_at = lax.axis_index("c")
    rows = lax.all_to_all(
        jnp.broadcast_to(residual_in, (ZY, count, width)), ("z", "y"), 0, 0, tiled=True
    )
    own = jnp.concatenate([w_query.T, w_key.T, w_value.T, w_outgate.T], axis=0)
    mine = [own] + [
        lax.ppermute(own, "x", [(i, (i + shift) % 4) for i in range(4)]) for shift in (1, 2, 3)
    ]
    mine = jnp.stack(mine)
    other = swap_cores(mine)
    order = (x_at - jnp.arange(4)) % 4
    both = jnp.stack([mine[order], other[order]], axis=1)
    both = jnp.where(c_at == 0, both, both[:, ::-1])
    head_weights = both.reshape(4, 2, 4, 16, width).transpose(2, 0, 1, 3, 4).reshape(4 * HD, width)

    gate_other = swap_cores(w_gate)
    up_other = swap_cores(w_up)
    down_other = swap_cores(w_down)

    rows_first = rows.reshape(ZY * count, width).astype(jnp.float32)
    rows_normed = (rms_scale(rows_first) * gain_mix_pre).astype(jnp.bfloat16)
    columns = lax.dot_general(
        rows_normed, head_weights, (((1,), (1,)), ((), ())), preferred_element_type=jnp.float32
    ).astype(jnp.bfloat16)
    joined = lax.all_to_all(
        columns.reshape(ZY, count, 4 * HD), ("z", "y"), 0, 0, tiled=True
    )
    joined = joined.reshape(ZY, count, 4, HD).transpose(2, 1, 0, 3).reshape(4, count, H * HD)

    x_first = residual_in.astype(jnp.float32)
    normed = (rms_scale(x_first) * gain_mix_pre).astype(jnp.bfloat16)
    decay_in = jnp.dot(normed, w_decay, preferred_element_type=jnp.float32)
    beta_in = jnp.dot(normed, w_beta, preferred_element_type=jnp.float32)
    mixed, new_state = delta_step(
        joined[0],
        joined[1],
        joined[2],
        joined[3],
        decay_in,
        beta_in,
        state_cache,
        decay_scale,
        decay_bias,
        head_gain,
    )
    branch = jnp.dot(mixed, w_out, preferred_element_type=jnp.float32)
    x_second = x_first + rms_scale(branch) * gain_mix_post
    normed_two = (rms_scale(x_second) * gain_ffn_pre).astype(jnp.bfloat16)
    table = dispatch_table(routes, EXPERTS, CAP)
    picks = jnp.sum(table, axis=1)
    run = width // QUART
    placed = jnp.broadcast_to(
        picks.reshape(count, EXPERTS, 1, CAP), (count, EXPERTS, 2, CAP)
    ).reshape(count, CHIPS * CAP)
    choose = (
        placed.T[:, None, :, None] * jnp.eye(QUART, dtype=jnp.float32)[None, :, None, :]
    ).reshape(CHIPS * CAP * QUART, count * QUART)
    sent = jnp.dot(
        choose.astype(jnp.bfloat16),
        normed_two.reshape(count * QUART, run),
        preferred_element_type=jnp.float32,
    ).astype(jnp.bfloat16)
    block = lax.all_to_all(
        sent.reshape(CHIPS, CAP * QUART, run), ("z", "y", "x"), 0, 0, tiled=True
    )
    flat = block.reshape(CHIPS * CAP, width)

    def hidden_of(gate, upper):
        return clamped_unit(
            jnp.dot(flat, gate, preferred_element_type=jnp.float32),
            jnp.dot(flat, upper, preferred_element_type=jnp.float32),
        ).astype(jnp.bfloat16)

    partial_value = (
        jnp.dot(hidden_of(w_gate, w_up), w_down, preferred_element_type=jnp.float32)
        + jnp.dot(hidden_of(gate_other, up_other), down_other, preferred_element_type=jnp.float32)
    ).astype(jnp.bfloat16)
    returned = lax.all_to_all(
        partial_value.reshape(CHIPS, CAP * QUART, run), ("z", "y", "x"), 0, 0, tiled=True
    )
    summed = jnp.sum(returned.reshape(EXPERTS, 2, CAP, width).astype(jnp.float32), axis=1)
    summed = summed.reshape(EXPERTS * CAP, width)
    raised = jnp.exp(route_logits)
    weights = raised / jnp.sum(raised, axis=-1, keepdims=True)
    mix_table = jnp.einsum("ske,sk->se", table, weights)
    moe = jnp.dot(mix_table, summed)
    result = (x_second + rms_scale(moe) * gain_ffn_post).astype(jnp.bfloat16)
    return (result, new_state)


def solution(mesh):
    torus = Mesh(mesh.devices.reshape(4, 4, 4, 2), ("z", "y", "x", "c"))
    ep = ("z", "y", "x", "c")
    in_specs = (
        P(ep, None),
        P(),
        P(None, ep),
        P(None, ep),
        P(None, ep),
        P(None, ep),
        P(),
        P(),
        P(),
        P(),
        P(),
        P(),
        P(),
        P(ep, None, None, None),
        P(),
        P(ep, None),
        P(ep, None),
        P(None, ep),
        P(None, ep),
        P(ep, None),
        P(),
    )
    out_specs = (P(ep, None), P(ep, None, None, None))
    return jax.shard_map(
        shards, mesh=torus, in_specs=in_specs, out_specs=out_specs, check_vma=False
    )
```

time: 188 us -> 113 us (0.60)
  waiting for transfers between devices: 107 us -> 32 us
  starting transfers between devices: 16 us -> 32.4 us
  between operations: 14.3 us -> 1.08 us
    all_gather x1 -> x0, waiting for transfers between devices: 66.2 us -> none  [shards(): lax.all_gather(normed, 'ep', axis=0, tiled=True)]
    all_to_all x3 -> x4, waiting for transfers between devices: 40.9 us -> 30.8 us  [the longest x1 12.1 us: shards(): lax.all_to_all(sent.reshape(CHIPS, CAP * QUART, run), ('z', 'y', 'x'), 0,...]
    all_to_all x3 -> x4, starting transfers between devices: 15.9 us -> 24.7 us  [the longest x1 8.05 us: shards(): lax.all_to_all(jnp.broadcast_to(residual_in, (ZY, count, width)), ('z', '...]
    ppermute x0 -> x7, starting transfers between devices: none -> 7.64 us  [the longest x3 6.45 us: shards(): lax.ppermute(own, 'x', [(i, (i + shift) % 4) for i in range(4)])]
    dot_general x3 -> x6, matrix products: 7.05 us -> 12.8 us  [the longest x2 4.08 us: hidden_of(): jnp.dot(flat, gate, preferred_element_type=jnp.float32)]
    unnamed x1 -> x0, matrix products: 3.58 us -> none
    unnamed x19 -> x29, local copies, waits for them, and re-layouts: 3.03 us -> 0.29 us
    gather x0 -> x2, local copies, waits for them, and re-layouts: none -> 2.45 us  [shards(): both = jnp.stack([mine[order], other[order]], axis=1)]
  transfers between devices with their start and end apart: 4 -> 11, of which waited for: 4 -> 5; matrix products, arithmetic and copies ran while one was open for 6% -> 35% of each run, Pallas kernels for 0% -> 0%
where the time goes in v1:
time: 113 us
  starting transfers between devices  32.4 us (29%)
  waiting for transfers between devices  32 us (28%)
  matrix products  25.8 us (23%)
  other arithmetic  11.5 us (10%)
  local copies, waits for them, and re-layouts  9.87 us (9%)
    all_to_all x1, waiting for transfers between devices, shards(): lax.all_to_all(sent.reshape(CHIPS, CAP * QUART, run), ('z', 'y', 'x'), 0,...  12.1 us
    all_to_all x1, starting transfers between devices, shards(): lax.all_to_all(jnp.broadcast_to(residual_in, (ZY, count, width)), ('z', '...  8.05 us
    all_to_all x1, waiting for transfers between devices, shards(): lax.all_to_all(columns.reshape(ZY, count, 4 * HD), ('z', 'y'), 0, 0, tile...  7.76 us
    all_to_all x1, starting transfers between devices, shards(): lax.all_to_all(columns.reshape(ZY, count, 4 * HD), ('z', 'y'), 0, 0, tile...  7.14 us
    ppermute x3, starting transfers between devices, shards(): lax.ppermute(own, 'x', [(i, (i + shift) % 4) for i in range(4)])  6.45 us
    convert_element_type x1, other arithmetic, delta_step(): return (gated.astype(jnp.bfloat16), held.astype(jnp.bfloat16))  5.95 us
    all_to_all x1, waiting for transfers between devices, shards(): lax.all_to_all(partial_value.reshape(CHIPS, CAP * QUART, run), ('z', 'y',...  5.89 us
    all_to_all x1, waiting for transfers between devices, shards(): lax.all_to_all(jnp.broadcast_to(residual_in, (ZY, count, width)), ('z', '...  5.05 us
  transfers between devices with their start and end apart: 11, of which 5 were waited for; matrix products, arithmetic and copies ran while one was open for 35% of the time, Pallas kernels for 0%

profile of v1, /device:TPU:0, one launch (start us, length us, event | category | flops | bytes accessed | tf_op | source)
XLA Modules:
  0.0 112.6 jit_solution(17935695650156131213)
XLA Ops:
  1.7 3.2 %collective-permute-start.1 = (bf16[64,2048]{1,0:T(8,128)(2,1)S(1)}, bf16[64,2048]{1,0:T(8,128)(2,1)S(1)}, u32[]{:S(2)}, u32[]{:S(2)}) collective-permute-start(bf16[64,2048]{1,0:T(8,128)(2,1)S(1)} %get-tuple-element.5), channel_id=1, source_target_pairs={{0,4},{2,6},{4,0},{6,2},{1,5},{3,7},{5,1},{7,3},{8,12},{10,14},{12... | collective-permute-start | bytes 786440 | tf_op jit(solution)/shard_map/ppermute | solution.py:99
  5.5 2.6 %collective-permute-start.2 = (bf16[64,2048]{1,0:T(8,128)(2,1)S(1)}, bf16[64,2048]{1,0:T(8,128)(2,1)S(1)}, u32[]{:S(2)}, u32[]{:S(2)}) collective-permute-start(bf16[64,2048]{1,0:T(8,128)(2,1)S(1)} %get-tuple-element.5), channel_id=1, source_target_pairs={{0,6},{2,0},{4,2},{6,4},{1,7},{3,1},{5,3},{7,5},{8,14},{10,8},{12,... | collective-permute-start | bytes 786440 | tf_op jit(solution)/shard_map/ppermute | solution.py:99
  8.2 1.6 %broadcast_in_dim.6 = bf16[16,8,2048]{2,1,0:T(8,128)(2,1)} broadcast(bf16[8,2048]{1,0:T(8,128)(2,1)} %param.21), dimensions={1,2} | broadcast | bytes 557056 | tf_op jit(solution)/shard_map/broadcast_in_dim | solution.py:95
  9.8 8.0 %all-to-all-start = ((bf16[16,8,2048]{2,1,0:T(8,128)(2,1)}), bf16[16,8,2048]{2,1,0:T(8,128)(2,1)S(1)}, u32[]{:S(2)}, u32[]{:S(2)}) async-start(bf16[16,8,2048]{2,1,0:T(8,128)(2,1)} %broadcast_in_dim.6), calls=%async_computation | async-start | bytes 1048576 | tf_op jit(solution)/shard_map/all_to_all | solution.py:94
  20.9 2.0 %convert_element_type.126 = bf16[512,32]{0,1:T(8,128)(2,1)S(1)} reshape(bf16[128,4,8,4]{1,0,3,2:T(8,128)(2,1)S(1)} %multiply_convert_fusion) | data formatting | bytes 65536 | tf_op jit(solution)/shard_map/convert_element_type | solution.py:151
  23.5 5.1 %all-to-all-done = bf16[16,8,2048]{2,1,0:T(8,128)(2,1)S(1)} async-done(((bf16[16,8,2048]{2,1,0:T(8,128)(2,1)}), bf16[16,8,2048]{2,1,0:T(8,128)(2,1)S(1)}, u32[]{:S(2)}, u32[]{:S(2)}) %all-to-all-start) | async-done | bytes 524320 | tf_op jit(solution)/shard_map/all_to_all | solution.py:94
  28.8 1.1 %collective-permute-done.3 = bf16[4,64,2048]{2,1,0:T(8,128)(2,1)} collective-permute-done((bf16[4,64,2048]{2,1,0:T(8,128)(2,1)S(1)}, bf16[4,64,2048]{2,1,0:T(8,128)(2,1)}, u32[]{:S(2)}, u32[]{:S(2)}) %collective-permute-start.3) | collective-permute-done | bytes 1048608 | tf_op jit(solution)/shard_map/ppermute | solution.py:65
  29.9 1.8 %gather_fusion.1 = bf16[4,64,2048]{2,1,0:T(8,128)(2,1)S(1)} fusion(bf16[4,64,2048]{2,1,0:T(8,128)(2,1)} %collective-permute-done.3, s32[1024]{0:T(1024)S(1)} %pad_clamp_fusion), kind=kCustom, calls=%fused_computation.1 | custom fusion | bytes 2097168 | tf_op jit(solution)/shard_map/gather | solution.py:104
  32.8 1.5 %fusion.13 = bf16[16,8,512]{2,1,0:T(8,128)(2,1)} fusion(bf16[512,2048]{1,0:T(8,128)(2,1)S(1)} %bitcast.125, bf16[16,8,2048]{2,1,0:T(8,128)(2,1)S(1)} %all-to-all-done, f32[2048]{0:T(1024)S(1)} %copy-done.10, f32[16,8]{1,0:T(8,128)S(1)} %add_rsqrt_fusion), kind=kOutput, calls=%fused_computation.29 | convolution fusion | flops 269549568 | bytes 2761216 | tf_op jit(solution)/shard_map/dot_general | solution.py:114
  34.3 7.1 %all-to-all-start.1 = ((bf16[16,8,512]{2,1,0:T(8,128)(2,1)}), bf16[16,8,512]{2,1,0:T(8,128)(2,1)S(1)}, u32[]{:S(2)}, u32[]{:S(2)}) async-start(bf16[16,8,512]{2,1,0:T(8,128)(2,1)} %fusion.13), calls=%async_computation.1 | async-start | bytes 262144 | tf_op jit(solution)/shard_map/all_to_all | solution.py:117
  41.7 7.8 %all-to-all-done.1 = bf16[16,8,512]{2,1,0:T(8,128)(2,1)S(1)} async-done(((bf16[16,8,512]{2,1,0:T(8,128)(2,1)}), bf16[16,8,512]{2,1,0:T(8,128)(2,1)S(1)}, u32[]{:S(2)}, u32[]{:S(2)}) %all-to-all-start.1) | async-done | bytes 131104 | tf_op jit(solution)/shard_map/all_to_all | solution.py:117
  50.0 3.6 %fusion = f32[8,16,1,128]{3,2,1,0:T(1,128)S(1)} fusion(bf16[8,16,128,128]{3,2,1,0:T(8,128)(2,1)} %param.34, f32[8,16]{1,0:T(8,128)S(1)} %fusion.73, bf16[8,16,128,1]{2,0,1,3:T(8,128)(2,1)S(1)} %get-tuple-element.7), kind=kOutput, calls=%fused_computation.4 | convolution fusion | flops 8388608 | bytes 4293120 | tf_op jit(solution)/shard_map/rhk,rhkv->rhv/dot_general | solution.py:56
  53.8 3.8 %fusion.2 = f32[8,16,1,128]{3,2,1,0:T(1,128)S(1)} fusion(bf16[8,16,128,128]{3,2,1,0:T(8,128)(2,1)S(1)} %copy-done.1, f32[8,16,128]{2,1,0:T(8,128)S(1)} %copy.76, f32[8,16,128]{2,1,0:T(8,128)S(1)} %copy.74, f32[8,16]{1,0:T(8,128)S(1)} %fusion.73, bf16[8,16,128,1]{2,0,1,3:T(8,128)(2,1)S(1)} %get-tuple-element.6), kind=kOutput, calls=%fused_computation.6 | convolution fusion | flops 12582912 | bytes 4424192 | tf_op jit(solution)/shard_map/rhk,rhkv->rhv/dot_general | solution.py:58
  57.9 4.8 %multiply_reduce_fusion.2 = (f32[8]{0:T(128)S(1)}, f32[8,2048]{1,0:T(8,128)S(1)}) fusion(bf16[2048,2048]{1,0:T(8,128)(2,1)} %param.32, f32[8,16,1,128]{3,2,1,0:T(1,128)S(1)} %fusion.2, bf16[4,8,16,128]{3,1,0,2:T(8,128)(2,1)S(1)} %bitcast.129, f32[128]{0:T(128)S(1)} %copy-done.8, f32[8,16]{0,1:T(8,128)S(1)} %copy.78), kind=kOutput, calls=%fused_computation.98 | convolution fusion | flops 67289080 | bytes 8561184 | tf_op jit(solution)/shard_map/dot_general | solution.py:138
  63.0 1.1 fusion.8
  64.1 4.8 %all-to-all-start.2 = ((bf16[64,8,512]{2,1,0:T(8,128)(2,1)}), bf16[64,8,512]{2,1,0:T(8,128)(2,1)S(1)}, u32[]{:S(2)}, u32[]{:S(2)}) async-start(bf16[64,8,512]{2,1,0:T(8,128)(2,1)} %fusion.8), calls=%async_computation.2 | async-start | bytes 1048576 | tf_op jit(solution)/shard_map/all_to_all | solution.py:155
  69.2 12.1 %all-to-all-done.2 = bf16[64,8,512]{2,1,0:T(8,128)(2,1)S(1)} async-done(((bf16[64,8,512]{2,1,0:T(8,128)(2,1)}), bf16[64,8,512]{2,1,0:T(8,128)(2,1)S(1)}, u32[]{:S(2)}, u32[]{:S(2)}) %all-to-all-start.2) | async-done | bytes 524320 | tf_op jit(solution)/shard_map/all_to_all | solution.py:155
  81.6 2.0 %convolution_minimum_fusion.1 = f32[128,512]{1,0:T(8,128)S(1)} fusion(bf16[128,2048]{1,0:T(8,128)(2,1)S(1)} %reshape.238, bf16[2048,512]{1,0:T(8,128)(2,1)} %param.38), kind=kOutput, calls=%fused_computation.23 | convolution fusion | flops 268500992 | bytes 2883584 | tf_op jit(solution)/shard_map/dot_general | solution.py:162
  83.6 3.1 %fusion.14 = f32[128,2048]{1,0:T(8,128)S(1)} fusion(bf16[512,2048]{1,0:T(8,128)(2,1)} %param.40, bf16[128,2048]{1,0:T(8,128)(2,1)S(1)} %reshape.238, bf16[2048,512]{1,0:T(8,128)(2,1)} %param.39, f32[128,512]{1,0:T(8,128)S(1)} %convolution_minimum_fusion.1), kind=kOutput, calls=%fused_computation.30 | convolution fusion | flops 537460736 | bytes 6029312 | tf_op jit(solution)/shard_map/dot_general | solution.py:167
  86.7 2.0 %convolution_minimum_fusion = f32[128,512]{1,0:T(8,128)S(1)} fusion(bf16[128,2048]{1,0:T(8,128)(2,1)S(1)} %reshape.238, bf16[2048,512]{1,0:T(8,128)(2,1)} %collective-permute-done.4), kind=kOutput, calls=%fused_computation.21 | convolution fusion | flops 268500992 | bytes 2883584 | tf_op jit(solution)/shard_map/dot_general | solution.py:162
  88.8 3.1 %fusion.7 = bf16[128,2048]{1,0:T(8,128)(2,1)S(1)} fusion(f32[128,2048]{1,0:T(8,128)S(1)} %fusion.14, bf16[512,2048]{1,0:T(8,128)(2,1)} %collective-permute-done.6, f32[128,512]{1,0:T(8,128)S(1)} %convolution_minimum_fusion, bf16[128,2048]{1,0:T(8,128)(2,1)S(1)} %reshape.238, bf16[2048,512]{1,0:T(8,128)(2,1)} %collective-permute-done.5), kind=kOutput, calls=%fused_computation.13 | convolution fusion | flops 537985024 | bytes 6553600 | tf_op jit(solution)/shard_map/dot_general | solution.py:168
  93.0 4.7 %all-to-all-start.3 = ((bf16[64,8,512]{2,1,0:T(8,128)(2,1)}), bf16[64,8,512]{2,1,0:T(8,128)(2,1)S(1)}, u32[]{:S(2)}, u32[]{:S(2)}) async-start(bf16[64,8,512]{2,1,0:T(8,128)(2,1)} %reshape.239), calls=%async_computation.3 | async-start | bytes 1048576 | tf_op jit(solution)/shard_map/all_to_all | solution.py:170
  97.8 5.9 %fusion.1 = bf16[8,16,128,128]{3,2,1,0:T(8,128)(2,1)} fusion(bf16[8,16,128,128]{3,2,1,0:T(8,128)(2,1)} %param.34, f32[8,16,128]{2,1,0:T(8,128)S(1)} %copy.76, f32[8,16,128]{2,1,0:T(8,128)S(1)} %copy.74, f32[8,16]{1,0:T(8,128)S(1)} %fusion.73), kind=kLoop, calls=%fused_computation.5 | loop fusion | flops 10485760 | bytes 8520192 | tf_op jit(solution)/shard_map/convert_element_type | solution.py:61
  103.8 5.9 %all-to-all-done.3 = bf16[64,8,512]{2,1,0:T(8,128)(2,1)S(1)} async-done(((bf16[64,8,512]{2,1,0:T(8,128)(2,1)}), bf16[64,8,512]{2,1,0:T(8,128)(2,1)S(1)}, u32[]{:S(2)}, u32[]{:S(2)}) %all-to-all-start.3) | async-done | bytes 524320 | tf_op jit(solution)/shard_map/all_to_all | solution.py:170
  (100 shorter events, 12.6 us)
Async XLA Ops:
  0.6 18.6 %copy-start = (bf16[2048,16]{0,1:T(8,128)(2,1)S(1)}, bf16[2048,16]{0,1:T(8,128)(2,1)}, u32[]{:S(2)}) copy-start(bf16[2048,16]{0,1:T(8,128)(2,1)} %param.28) | copy-start | bytes 196612
  0.6 17.8 %copy-start.2 = (bf16[8,2048]{1,0:T(8,128)(2,1)S(1)}, bf16[8,2048]{1,0:T(8,128)(2,1)}, u32[]{:S(2)}) copy-start(bf16[8,2048]{1,0:T(8,128)(2,1)} %param.21) | copy-start | bytes 98308
  0.7 17.9 %copy-start.7 = (s32[8,4]{0,1:T(4,128)S(1)}, s32[8,4]{0,1:T(4,128)}, u32[]{:S(2)}) copy-start(s32[8,4]{0,1:T(4,128)} %param.36) | copy-start | bytes 388
  0.7 18.6 %copy-start.10 = (f32[2048]{0:T(1024)S(1)}, f32[2048]{0:T(1024)}, u32[]{:S(2)}) copy-start(f32[2048]{0:T(1024)} %param.22) | copy-start | bytes 24580
  1.7 18.6 %copy-start.11 = (f32[16]{0:T(128)S(1)}, f32[16]{0:T(128)}, u32[]{:S(2)}) copy-start(f32[16]{0:T(128)} %param.29) | copy-start | bytes 196
  1.7 17.7 %collective-permute-start.1 = (bf16[64,2048]{1,0:T(8,128)(2,1)S(1)}, bf16[64,2048]{1,0:T(8,128)(2,1)S(1)}, u32[]{:S(2)}, u32[]{:S(2)}) collective-permute-start(bf16[64,2048]{1,0:T(8,128)(2,1)S(1)} %get-tuple-element.5), channel_id=1, source_target_pairs={{0,4},{2,6},{4,0},{6,2},{1,5},{3,7},{5,1},{7,3},{8,12},{10,14},{12... | collective-permute-start | bytes 786440 | tf_op jit(solution)/shard_map/ppermute | solution.py:99
  4.9 14.6 %collective-permute-start = (bf16[64,2048]{1,0:T(8,128)(2,1)S(1)}, bf16[64,2048]{1,0:T(8,128)(2,1)S(1)}, u32[]{:S(2)}, u32[]{:S(2)}) collective-permute-start(bf16[64,2048]{1,0:T(8,128)(2,1)S(1)} %get-tuple-element.5), channel_id=1, source_target_pairs={{0,2},{2,4},{4,6},{6,0},{1,3},{3,5},{5,7},{7,1},{8,10},{10,12},{12... | collective-permute-start | bytes 786440 | tf_op jit(solution)/shard_map/ppermute | solution.py:99
  5.5 14.0 %collective-permute-start.2 = (bf16[64,2048]{1,0:T(8,128)(2,1)S(1)}, bf16[64,2048]{1,0:T(8,128)(2,1)S(1)}, u32[]{:S(2)}, u32[]{:S(2)}) collective-permute-start(bf16[64,2048]{1,0:T(8,128)(2,1)S(1)} %get-tuple-element.5), channel_id=1, source_target_pairs={{0,6},{2,0},{4,2},{6,4},{1,7},{3,1},{5,3},{7,5},{8,14},{10,8},{12,... | collective-permute-start | bytes 786440 | tf_op jit(solution)/shard_map/ppermute | solution.py:99
  9.8 18.8 %all-to-all-start = ((bf16[16,8,2048]{2,1,0:T(8,128)(2,1)}), bf16[16,8,2048]{2,1,0:T(8,128)(2,1)S(1)}, u32[]{:S(2)}, u32[]{:S(2)}) async-start(bf16[16,8,2048]{2,1,0:T(8,128)(2,1)} %broadcast_in_dim.6), calls=%async_computation | async-start | bytes 1048576 | tf_op jit(solution)/shard_map/all_to_all | solution.py:94
  17.8 68.9 %collective-permute-start.4 = (bf16[2048,512]{1,0:T(8,128)(2,1)}, bf16[2048,512]{1,0:T(8,128)(2,1)}, u32[]{:S(2)}, u32[]{:S(2)}) collective-permute-start(bf16[2048,512]{1,0:T(8,128)(2,1)} %param.38), channel_id=1, source_target_pairs={{0,1},{1,0},{2,3},{3,2},{4,5},{5,4},{6,7},{7,6},{8,9},{9,8},{10,11... | collective-permute-start | bytes 6291464 | tf_op jit(solution)/shard_map/ppermute | solution.py:65
  17.9 70.9 %collective-permute-start.5 = (bf16[2048,512]{1,0:T(8,128)(2,1)}, bf16[2048,512]{1,0:T(8,128)(2,1)}, u32[]{:S(2)}, u32[]{:S(2)}) collective-permute-start(bf16[2048,512]{1,0:T(8,128)(2,1)} %param.39), channel_id=1, source_target_pairs={{0,1},{1,0},{2,3},{3,2},{4,5},{5,4},{6,7},{7,6},{8,9},{9,8},{10,11... | collective-permute-start | bytes 6291464 | tf_op jit(solution)/shard_map/ppermute | solution.py:65
  19.4 69.4 %collective-permute-start.6 = (bf16[512,2048]{1,0:T(8,128)(2,1)}, bf16[512,2048]{1,0:T(8,128)(2,1)}, u32[]{:S(2)}, u32[]{:S(2)}) collective-permute-start(bf16[512,2048]{1,0:T(8,128)(2,1)} %param.40), channel_id=1, source_target_pairs={{0,1},{1,0},{2,3},{3,2},{4,5},{5,4},{6,7},{7,6},{8,9},{9,8},{10,11... | collective-permute-start | bytes 6291464 | tf_op jit(solution)/shard_map/ppermute | solution.py:65
  19.7 10.2 %collective-permute-start.3 = (bf16[4,64,2048]{2,1,0:T(8,128)(2,1)S(1)}, bf16[4,64,2048]{2,1,0:T(8,128)(2,1)}, u32[]{:S(2)}, u32[]{:S(2)}) collective-permute-start(bf16[4,64,2048]{2,1,0:T(8,128)(2,1)S(1)} %pad_maximum_fusion.1), channel_id=1, source_target_pairs={{0,1},{1,0},{2,3},{3,2},{4,5},{5,4},{6,7},{7,6},{8,9},{9,8},{10,11... | collective-permute-start | bytes 3145736 | tf_op jit(solution)/shard_map/ppermute | solution.py:65
  32.8 8.7 %copy-start.9 = (bf16[2048,16]{0,1:T(8,128)(2,1)S(1)}, bf16[2048,16]{0,1:T(8,128)(2,1)}, u32[]{:S(2)}) copy-start(bf16[2048,16]{0,1:T(8,128)(2,1)} %param.27) | copy-start | bytes 196612
  32.8 8.7 %copy-start.12 = (f32[16]{0:T(128)S(1)}, f32[16]{0:T(128)}, u32[]{:S(2)}) copy-start(f32[16]{0:T(128)} %param.30) | copy-start | bytes 196
  34.3 15.1 %all-to-all-start.1 = ((bf16[16,8,512]{2,1,0:T(8,128)(2,1)}), bf16[16,8,512]{2,1,0:T(8,128)(2,1)S(1)}, u32[]{:S(2)}, u32[]{:S(2)}) async-start(bf16[16,8,512]{2,1,0:T(8,128)(2,1)} %fusion.13), calls=%async_computation.1 | async-start | bytes 262144 | tf_op jit(solution)/shard_map/all_to_all | solution.py:117
  50.0 3.8 %copy-start.1 = (bf16[8,16,128,128]{3,2,1,0:T(8,128)(2,1)S(1)}, bf16[8,16,128,128]{3,2,1,0:T(8,128)(2,1)}, u32[]{:S(2)}) copy-start(bf16[8,16,128,128]{3,2,1,0:T(8,128)(2,1)} %param.34) | copy-start | bytes 12582916
  53.8 4.1 %copy-start.8 = (f32[128]{0:T(128)S(1)}, f32[128]{0:T(128)}, u32[]{:S(2)}) copy-start(f32[128]{0:T(128)} %param.31) | copy-start | bytes 1540
  57.9 4.8 %copy-start.3 = (f32[2048]{0:T(1024)S(1)}, f32[2048]{0:T(1024)}, u32[]{:S(2)}) copy-start(f32[2048]{0:T(1024)} %param.33) | copy-start | bytes 24580
  57.9 5.0 %copy-start.4 = (f32[2048]{0:T(1024)S(1)}, f32[2048]{0:T(1024)}, u32[]{:S(2)}) copy-start(f32[2048]{0:T(1024)} %param.35) | copy-start | bytes 24580
  57.9 11.1 %copy-start.5 = (f32[8,4]{0,1:T(4,128)S(1)}, f32[8,4]{0,1:T(4,128)}, u32[]{:S(2)}) copy-start(f32[8,4]{0,1:T(4,128)} %param.37) | copy-start | bytes 388
  64.1 17.2 %all-to-all-start.2 = ((bf16[64,8,512]{2,1,0:T(8,128)(2,1)}), bf16[64,8,512]{2,1,0:T(8,128)(2,1)S(1)}, u32[]{:S(2)}, u32[]{:S(2)}) async-start(bf16[64,8,512]{2,1,0:T(8,128)(2,1)} %fusion.8), calls=%async_computation.2 | async-start | bytes 1048576 | tf_op jit(solution)/shard_map/all_to_all | solution.py:155
  93.0 16.7 %all-to-all-start.3 = ((bf16[64,8,512]{2,1,0:T(8,128)(2,1)}), bf16[64,8,512]{2,1,0:T(8,128)(2,1)S(1)}, u32[]{:S(2)}, u32[]{:S(2)}) async-start(bf16[64,8,512]{2,1,0:T(8,128)(2,1)} %reshape.239), calls=%async_computation.3 | async-start | bytes 1048576 | tf_op jit(solution)/shard_map/all_to_all | solution.py:170
  103.8 8.1 %copy-start.6 = (f32[2048]{0:T(1024)S(1)}, f32[2048]{0:T(1024)}, u32[]{:S(2)}) copy-start(f32[2048]{0:T(1024)} %param.41) | copy-start | bytes 24580

commit v2 on v1

v2 whole, which is shorter than its diff:
```python
import jax
import jax.numpy as jnp
from jax import lax
from jax.experimental import pallas as pl
from jax.experimental.pallas import tpu as pltpu
from jax.sharding import Mesh
from jax.sharding import PartitionSpec as P


H = 16
HD = 128
D = 2048
TOPK = 4
EXPERTS = 32
CAP = 2
SEQ = 8
ZY = 16
CHIPS = 64
QUART = 4
RUN = D // QUART
LINES = CHIPS * CAP * QUART
ROWS = CHIPS * CAP


EPS = 1e-06
LIMIT = 7.0
ALPHA = 1.702

F32 = jnp.float32
BF16 = jnp.bfloat16
MIB = 1 << 20


def iota(shape, dimension):
    return lax.broadcasted_iota(jnp.int32, shape, dimension)


def nt(left, right):
    return lax.dot_general(left, right, (((1,), (1,)), ((), ())), preferred_element_type=F32)


def mm(left, right):
    return jnp.dot(left, right, preferred_element_type=F32)


def silu(values):
    return values * jax.nn.sigmoid(values)


def rms_scale(values):
    return values * lax.rsqrt(jnp.mean(values * values, axis=-1, keepdims=True) + EPS)


def halves(values):
    high = values.astype(BF16)
    return high, (values - high.astype(F32)).astype(BF16)


def clamped_unit(gate, upper):
    glu = jnp.minimum(gate, LIMIT)
    linear = jnp.clip(upper, -LIMIT, LIMIT)
    return glu * jax.nn.sigmoid(ALPHA * glu) * (linear + 1.0)


def call(body, outs, limit, scratch=(), specs=None, outs_specs=None, flops=0):
    return pl.pallas_call(
        body,
        out_shape=outs,
        **({} if specs is None else {"in_specs": specs}),
        **({} if outs_specs is None else {"out_specs": outs_specs}),
        scratch_shapes=list(scratch),
        compiler_params=pltpu.CompilerParams(vmem_limit_bytes=limit * MIB),
        cost_estimate=pl.CostEstimate(flops=flops, bytes_accessed=0, transcendentals=0),
    )


def shape(dims, dtype):
    return jax.ShapeDtypeStruct(dims, dtype)


def route_body(
    routes_ref,
    logits_ref,
    x_ref,
    gain_pre_ref,
    decay_w_ref,
    beta_w_ref,
    scale_ref,
    bias_ref,
    send_ref,
    mix_ref,
    fade_ref,
    beta_ref,
):
    normed = (rms_scale(x_ref[...].astype(F32)) * gain_pre_ref[...]).astype(BF16)
    raised = nt(normed, decay_w_ref[...]) + bias_ref[...]
    soft = jnp.maximum(raised, 0.0) + jnp.log1p(jnp.exp(-jnp.abs(raised)))
    fade_ref[...] = jnp.exp(-scale_ref[...] * soft)
    beta_ref[...] = jax.nn.sigmoid(nt(normed, beta_w_ref[...]))
    routes = routes_ref[...]
    raised = jnp.exp(logits_ref[...])
    weights = raised / jnp.sum(raised, axis=-1, keepdims=True)
    named = iota((SEQ, EXPERTS), 1)
    hits = jnp.zeros((SEQ, EXPERTS), F32)
    weighed = jnp.zeros((SEQ, EXPERTS), F32)
    for j in range(TOPK):
        hit = (routes[:, j : j + 1] == named).astype(F32)
        hits = hits + hit
        weighed = weighed + hit * weights[:, j : j + 1]
    earlier = (iota((SEQ, SEQ), 0) > iota((SEQ, SEQ), 1)).astype(BF16)
    slots = mm(earlier, hits.astype(BF16))
    line = iota((LINES, EXPERTS), 0)
    expert_of = (line // (2 * CAP * QUART)) == iota((LINES, EXPERTS), 1)
    slot_of = (line // QUART) % CAP
    column = iota((LINES, QUART * SEQ), 1)
    same_run = (iota((LINES, QUART * SEQ), 0) % QUART) == (column // SEQ)
    send = jnp.zeros((LINES, QUART * SEQ), F32)
    mix = jnp.zeros((LINES, QUART * SEQ), F32)
    for slot in range(CAP):
        chosen = (expert_of & (slot_of == slot)).astype(BF16)
        here = slots == slot
        picks = jnp.where(here, hits, 0.0)
        shares = jnp.where(here, weighed, 0.0)
        high, low = halves(jnp.concatenate([shares] * QUART, axis=0))
        send = send + nt(chosen, jnp.concatenate([picks] * QUART, axis=0).astype(BF16))
        mix = mix + (nt(chosen, high) + nt(chosen, low))
    send_ref[...] = jnp.where(same_run, send, 0.0).astype(BF16)
    high, low = halves(jnp.where(same_run, mix, 0.0).T)
    mix_ref[...] = jnp.concatenate([high, low], axis=0)


def prepare_body(x_ref, q_ref, k_ref, v_ref, z_ref, rows_ref, own_ref, near_ref, wide_ref, sems):
    fetch = pltpu.make_async_copy(x_ref, near_ref, sems.at[4])
    fetch.start()
    copies = [
        pltpu.make_async_copy(ref, own_ref.at[pl.ds(i * 16, 16)], sems.at[i])
        for i, ref in enumerate((q_ref, k_ref, v_ref, z_ref))
    ]
    for copy in copies:
        copy.start()
    fetch.wait()
    for i in range(ZY):
        wide_ref[i] = near_ref[...]
    store = pltpu.make_async_copy(wide_ref, rows_ref, sems.at[5])
    store.start()
    for copy in copies:
        copy.wait()
    store.wait()


def head_body(
    at_ref, rows_ref, gain_ref, o0, o1, o2, o3, p0, p1, p2, p3, out_ref, weights_ref, near_ref, sem
):
    fetch = pltpu.make_async_copy(gain_ref, near_ref, sem)
    fetch.start()
    x_at = at_ref[0]
    c_at = at_ref[1]
    for shift, (own, other) in enumerate(zip((o0, o1, o2, o3), (p0, p1, p2, p3), strict=True)):
        place = ((x_at - shift) & 3) * 32
        for core, ref in ((c_at, own), (1 - c_at, other)):
            for kind in range(4):
                start = pl.multiple_of(kind * HD + place + core * 16, 16)
                weights_ref[pl.ds(start, 16), :] = ref[kind * 16 : kind * 16 + 16, :]
    scaled = rms_scale(rows_ref[...].astype(F32))
    fetch.wait()
    normed = (scaled * near_ref[...]).astype(BF16)
    out_ref[...] = nt(normed, weights_ref[...]).astype(BF16)


PARTS = 4


def mixer_body(
    joined_ref,
    x_ref,
    decay_ref,
    beta_ref,
    head_gain_ref,
    w_out_ref,
    gain_post_ref,
    gain_ffn_ref,
    send_ref,
    state_ref,
    sent_ref,
    second_ref,
    keys_ref,
    change_ref,
    fade_ref,
    mixed_ref,
    held_ref,
    held_out_ref,
    sems,
):
    held_in, out_in = [], []
    for i in range(PARTS):
        heads = pl.ds(i * (H // PARTS), H // PARTS)
        held_in.append(
            pltpu.make_async_copy(state_ref.at[:, heads], held_ref.at[:, heads], sems.at[i])
        )
        lines = pl.ds(i * (D // PARTS), D // PARTS)
        out_in.append(
            pltpu.make_async_copy(w_out_ref.at[lines], held_out_ref.at[lines], sems.at[PARTS + i])
        )
    for fetch in held_in + out_in:
        fetch.start()
    first = x_ref[...].astype(F32)
    fade = decay_ref[...]
    beta = beta_ref[...]
    turn = iota((4 * SEQ, HD), 0) % SEQ
    for head in range(H):
        if head % (H // PARTS) == 0:
            held_in[head // (H // PARTS)].wait()
        block = joined_ref[head].astype(F32)
        query = silu(block[:, :HD])
        query = query * (
            lax.rsqrt(jnp.sum(query * query, axis=-1, keepdims=True) + EPS) * HD ** (-0.5)
        )
        keys = silu(block[:, HD : 2 * HD])
        keys = keys * lax.rsqrt(jnp.sum(keys * keys, axis=-1, keepdims=True) + EPS)
        values = silu(block[:, 2 * HD : 3 * HD])
        left = jnp.concatenate([*halves(keys), *halves(query)], axis=0)
        both = jnp.zeros((4 * SEQ, HD), F32)
        for row in range(SEQ):
            both = jnp.where(turn == row, mm(left, held_ref[row, head]), both)
        faded = fade[:, head : head + 1]
        guess = faded * (both[:SEQ] + both[SEQ : 2 * SEQ])
        change = beta[:, head : head + 1] * (values - guess)
        output = faded * (both[2 * SEQ : 3 * SEQ] + both[3 * SEQ :])
        output = output + jnp.sum(query * keys, axis=-1, keepdims=True) * change
        output = rms_scale(output) * head_gain_ref[...] * silu(block[:, 3 * HD :])
        mixed_ref[:, head * HD : (head + 1) * HD] = output.astype(BF16)
        spot = slice(head * SEQ, (head + 1) * SEQ)
        keys_ref[spot, :] = keys
        change_ref[spot, :] = change
        fade_ref[spot, :] = jnp.broadcast_to(faded, (SEQ, HD))
    branch = jnp.zeros((SEQ, D), F32)
    for i in range(PARTS):
        out_in[i].wait()
        lines = slice(i * (D // PARTS), (i + 1) * (D // PARTS))
        branch = branch + mm(mixed_ref[:, lines], held_out_ref[lines, :])
    second = first + rms_scale(branch) * gain_post_ref[...]
    second_ref[...] = second
    normed_two = rms_scale(second) * gain_ffn_ref[...]
    runs = jnp.concatenate(
        [normed_two[:, i * RUN : (i + 1) * RUN] for i in range(QUART)], axis=0
    ).astype(BF16)
    sent_ref[...] = mm(send_ref[...], runs).astype(BF16)


HEADS = 2


def state_body(keys_ref, change_ref, fade_ref, state_ref, out_ref):
    for head in range(HEADS):
        spot = slice(head * SEQ, (head + 1) * SEQ)
        tall = keys_ref[spot, :].T
        for row in range(SEQ):
            at = head * SEQ + row
            held = state_ref[row, head].astype(F32) * fade_ref[at : at + 1, :]
            held = held + tall[:, row : row + 1] * change_ref[at : at + 1, :]
            out_ref[row, head] = held.astype(BF16)


def state_call(keys, change, fade, state):
    small = pl.BlockSpec((HEADS * SEQ, HD), lambda i: (i, 0))
    large = pl.BlockSpec((SEQ, HEADS, HD, HD), lambda i: (0, i, 0, 0))
    return pl.pallas_call(
        state_body,
        grid=(H // HEADS,),
        in_specs=[small, small, small, large],
        out_specs=large,
        out_shape=shape(state.shape, BF16),
        name="new_state",
        compiler_params=pltpu.CompilerParams(vmem_limit_bytes=8 * MIB),
        cost_estimate=pl.CostEstimate(flops=40_000_000, bytes_accessed=8 * MIB, transcendentals=0),
    )(keys, change, fade, state)


def expert_body(block_ref, g0, g1, u0, u1, d0, d1, out_ref):
    line = iota((LINES, LINES), 0)
    source = (line % ROWS) * QUART + line // ROWS
    gather = (iota((LINES, LINES), 1) == source).astype(BF16)
    runs = mm(gather, block_ref[...]).astype(BF16)
    rows = jnp.concatenate([runs[i * ROWS : (i + 1) * ROWS] for i in range(QUART)], axis=1)
    part = jnp.zeros((ROWS, D), F32)
    for gate_ref, up_ref, down_ref in ((g0, u0, d0), (g1, u1, d1)):
        hidden = clamped_unit(mm(rows, gate_ref[...]), mm(rows, up_ref[...])).astype(BF16)
        part = part + mm(hidden, down_ref[...])
    part = part.astype(BF16)
    runs = jnp.concatenate([part[:, i * RUN : (i + 1) * RUN] for i in range(QUART)], axis=0)
    back = (iota((LINES, LINES), 1) == (line % QUART) * ROWS + line // QUART).astype(BF16)
    out_ref[...] = mm(back, runs).astype(BF16)


def finish_body(back_ref, mix_ref, second_ref, gain_ref, out_ref):
    runs = mm(mix_ref[...], back_ref[...])
    runs = runs[: QUART * SEQ] + runs[QUART * SEQ :]
    moe = jnp.concatenate([runs[i * SEQ : (i + 1) * SEQ] for i in range(QUART)], axis=1)
    out_ref[...] = (second_ref[...] + rms_scale(moe) * gain_ref[...]).astype(BF16)


def swap_cores(values):
    return lax.ppermute(values, "c", [(0, 1), (1, 0)])


def exchange(values, axes):
    return lax.all_to_all(values, axes, 0, 0, tiled=True)


def shards(
    residual_in,
    gain_mix_pre,
    w_query,
    w_key,
    w_value,
    w_outgate,
    w_decay,
    w_beta,
    decay_scale,
    decay_bias,
    head_gain,
    w_out,
    gain_mix_post,
    state_cache,
    gain_ffn_pre,
    routes,
    route_logits,
    w_gate,
    w_up,
    w_down,
    gain_ffn_post,
):
    at = jnp.stack([lax.axis_index("x"), lax.axis_index("c")]).astype(jnp.int32)
    flat = lambda gain: gain.reshape(1, -1)
    vmem = pl.BlockSpec(memory_space=pltpu.VMEM)
    smem = pl.BlockSpec(memory_space=pltpu.SMEM)
    far = pl.BlockSpec(memory_space=pltpu.HBM)
    hbm = lambda value: pltpu.with_memory_space_constraint(value, pltpu.HBM)
    spread, own = call(
        prepare_body,
        (shape((ZY, SEQ, D), BF16), shape((64, D), BF16)),
        4,
        specs=[far] * 5,
        outs_specs=[far, vmem],
        scratch=[
            pltpu.VMEM((SEQ, D), BF16),
            pltpu.VMEM((ZY, SEQ, D), BF16),
            pltpu.SemaphoreType.DMA((6,)),
        ],
    )(*(hbm(value) for value in (residual_in, w_query.T, w_key.T, w_value.T, w_outgate.T)))
    rows = exchange(spread, ("z", "y"))
    mine = [own] + [
        lax.ppermute(own, "x", [(i, (i + shift) % 4) for i in range(4)]) for shift in (1, 2, 3)
    ]
    other = [swap_cores(one) for one in mine]
    gate_other = swap_cores(w_gate)
    up_other = swap_cores(w_up)
    down_other = swap_cores(w_down)

    columns = call(
        head_body,
        shape((ZY * SEQ, 4 * HD), BF16),
        6,
        scratch=[
            pltpu.VMEM((4 * HD, D), BF16),
            pltpu.VMEM((1, D), F32),
            pltpu.SemaphoreType.DMA,
        ],
        specs=[smem, vmem, far] + [vmem] * 8,
    )(at, rows.reshape(ZY * SEQ, D), hbm(flat(gain_mix_pre)), *mine, *other)
    joined = exchange(columns.reshape(ZY, SEQ, 4 * HD), ("z", "y"))
    send, mix, decay, beta = call(
        route_body,
        (
            shape((LINES, QUART * SEQ), BF16),
            shape((2 * QUART * SEQ, LINES), BF16),
            shape((SEQ, H), F32),
            shape((SEQ, H), F32),
        ),
        8,
    )(
        routes,
        route_logits,
        residual_in,
        flat(gain_mix_pre),
        w_decay.T,
        w_beta.T,
        flat(decay_scale),
        flat(decay_bias),
    )

    small = shape((H * SEQ, HD), F32)
    sent, second, keys, change, fade = call(
        mixer_body,
        (shape((LINES, RUN), BF16), shape((SEQ, D), F32), small, small, small),
        16,
        specs=[vmem] * 5 + [far] + [vmem] * 3 + [far],
        scratch=[
            pltpu.VMEM((SEQ, H * HD), BF16),
            pltpu.VMEM((SEQ, H, HD, HD), BF16),
            pltpu.VMEM((D, D), BF16),
            pltpu.SemaphoreType.DMA((2 * PARTS,)),
        ],
    )(
        joined,
        residual_in,
        decay,
        beta,
        flat(head_gain),
        hbm(w_out),
        flat(gain_mix_post),
        flat(gain_ffn_pre),
        send,
        hbm(state_cache),
    )
    block = exchange(sent.reshape(CHIPS, CAP * QUART, RUN), ("z", "y", "x"))
    new_state = state_call(keys, change, fade, hbm(state_cache))
    part = call(expert_body, shape((LINES, RUN), BF16), 20)(
        block.reshape(LINES, RUN), w_gate, gate_other, w_up, up_other, w_down, down_other
    )
    back = exchange(part.reshape(CHIPS, CAP * QUART, RUN), ("z", "y", "x"))
    result = call(finish_body, shape((SEQ, D), BF16), 8)(
        back.reshape(LINES, RUN), mix, second, flat(gain_ffn_post)
    )
    return (result, new_state)


def solution(mesh):
    torus = Mesh(mesh.devices.reshape(4, 4, 4, 2), ("z", "y", "x", "c"))
    ep = ("z", "y", "x", "c")
    in_specs = (
        P(ep, None),
        P(),
        P(None, ep),
        P(None, ep),
        P(None, ep),
        P(None, ep),
        P(),
        P(),
        P(),
        P(),
        P(),
        P(),
        P(),
        P(ep, None, None, None),
        P(),
        P(ep, None),
        P(ep, None),
        P(None, ep),
        P(None, ep),
        P(ep, None),
        P(),
    )
    out_specs = (P(ep, None), P(ep, None, None, None))
    return jax.shard_map(
        shards, mesh=torus, in_specs=in_specs, out_specs=out_specs, check_vma=False
    )
```

time: 113 us -> 108 us (0.956)
  Pallas kernels: 0 us -> 26 us
  matrix products: 25.8 us -> 0 us
  blocking collectives: 0 us -> 18.4 us
  other arithmetic: 11.5 us -> 0.07 us
  starting transfers between devices: 32.4 us -> 24.9 us
  local copies, waits for them, and re-layouts: 9.87 us -> 2.73 us
  waiting for transfers between devices: 32 us -> 33.7 us
    pallas_call x0 -> x7, Pallas kernels: none -> 26 us  [the longest x1 8.01 us: state_call(): pl.pallas_call(state_body, grid=(H // HEADS,), in_specs=[small, small, sm...]
    dot_general x13 -> x0, matrix products: 25.8 us -> none  [the longest x1 4.76 us: shards(): branch = jnp.dot(mixed, w_out, preferred_element_type=jnp.float32)]
    all_to_all x0 -> x1, blocking collectives: none -> 18.4 us  [exchange(): return lax.all_to_all(values, axes, 0, 0, tiled=True)]
    all_to_all x4 -> x3, waiting for transfers between devices: 30.8 us -> 21.7 us  [exchange(): return lax.all_to_all(values, axes, 0, 0, tiled=True)]
    all_to_all x4 -> x3, starting transfers between devices: 24.7 us -> 16.6 us  [exchange(): return lax.all_to_all(values, axes, 0, 0, tiled=True)]
    convert_element_type x6 -> x0, other arithmetic: 7.15 us -> none  [the longest x1 5.95 us: delta_step(): return (gated.astype(jnp.bfloat16), held.astype(jnp.bfloat16))]
    ppermute x3, waiting for transfers between devices: 0.01 us -> 7 us  [shards(): lax.ppermute(own, 'x', [(i, (i + shift) % 4) for i in range(4)])]
    ppermute x4 -> x7, waiting for transfers between devices: 1.16 us -> 5.06 us  [swap_cores(): return lax.ppermute(values, 'c', [(0, 1), (1, 0)])]
  transfers between devices with their start and end apart: 11 -> 13, of which waited for: 5 -> 5; matrix products, arithmetic and copies ran while one was open for 35% -> 0% of each run, Pallas kernels for 0% -> 18%
where the time goes in v2:
time: 108 us; the launch traced here: 107 us
  waiting for transfers between devices  33.7 us (31%)
  Pallas kernels  26 us (24%)
  starting transfers between devices  24.9 us (23%)
  blocking collectives  18.4 us (17%)
  local copies, waits for them, and re-layouts  2.73 us (3%)
    all_to_all x3, waiting for transfers between devices, exchange(): return lax.all_to_all(values, axes, 0, 0, tiled=True)  21.7 us
    all_to_all x1, blocking collectives, exchange(): return lax.all_to_all(values, axes, 0, 0, tiled=True)  18.4 us
    all_to_all x3, starting transfers between devices, exchange(): return lax.all_to_all(values, axes, 0, 0, tiled=True)  16.6 us
    pallas_call x1, Pallas kernels, state_call(): pl.pallas_call(state_body, grid=(H // HEADS,), in_specs=[small, small, sm...  8.01 us
    ppermute x3, waiting for transfers between devices, shards(): lax.ppermute(own, 'x', [(i, (i + shift) % 4) for i in range(4)])  7 us
    ppermute x3, starting transfers between devices, shards(): lax.ppermute(own, 'x', [(i, (i + shift) % 4) for i in range(4)])  6.6 us
    pallas_call x1, Pallas kernels, shards(): call(mixer_body, (shape((LINES, RUN), BF16), shape((SEQ, D), F32), small,...  5.73 us
    pallas_call x1, Pallas kernels, shards(): call(expert_body, shape((LINES, RUN), BF16), 20)  5.53 us
  transfers between devices with their start and end apart: 13, of which 5 were waited for; matrix products, arithmetic and copies ran while one was open for 0% of the time, Pallas kernels for 18%

profile of v2, /device:TPU:0, one launch (start us, length us, event | category | flops | bytes accessed | tf_op | source)
XLA Modules:
  0.0 106.8 jit_solution(4630278786125666201)
XLA Ops:
  0.7 0.5 collective-permute-start.8
  1.3 1.6 %shard_map.212 = (bf16[16,8,2048]{2,1,0:T(8,128)(2,1)}, bf16[64,2048]{1,0:T(8,128)(2,1)S(1)}) custom-call(bf16[8,2048]{1,0:T(8,128)(2,1)} %x_ref.5, bf16[16,2048]{1,0:T(8,128)(2,1)} %bitcast.35, bf16[16,2048]{1,0:T(8,128)(2,1)} %bitcast.36, bf16[16,2048]{1,0:T(8,128)(2,1)} %bitcast.37, bf16[16,2048]{1,0:T(8,128)(2,1)} %bitcast.38), custom_call_target="tpu_custom_call" | custom-call | tf_op jit(solution)/shard_map/pallas_call | solution.py:339
  3.0 0.5 collective-permute-start.3
  3.5 2.9 %collective-permute-start.2 = (bf16[64,2048]{1,0:T(8,128)(2,1)S(1)}, bf16[64,2048]{1,0:T(8,128)(2,1)S(1)}, u32[]{:S(2)}, u32[]{:S(2)}) collective-permute-start(bf16[64,2048]{1,0:T(8,128)(2,1)S(1)} %get-tuple-element.14.o0), channel_id=1, source_target_pairs={{0,6},{2,0},{4,2},{6,4},{1,7},{3,1},{5,3},{7,5},{8,14},{10,8},{12,... | collective-permute-start | bytes 786440 | tf_op jit(solution)/shard_map/ppermute | solution.py:353
  6.4 5.0 %collective-permute-done.3.p0 = bf16[64,2048]{1,0:T(8,128)(2,1)S(1)} collective-permute-done((bf16[64,2048]{1,0:T(8,128)(2,1)S(1)}, bf16[64,2048]{1,0:T(8,128)(2,1)S(1)}, u32[]{:S(2)}, u32[]{:S(2)}) %collective-permute-start.3) | collective-permute-done | bytes 262176 | tf_op jit(solution)/shard_map/ppermute | solution.py:303
  11.5 3.1 %collective-permute-start.1 = (bf16[64,2048]{1,0:T(8,128)(2,1)S(1)}, bf16[64,2048]{1,0:T(8,128)(2,1)S(1)}, u32[]{:S(2)}, u32[]{:S(2)}) collective-permute-start(bf16[64,2048]{1,0:T(8,128)(2,1)S(1)} %get-tuple-element.14.o0), channel_id=1, source_target_pairs={{0,4},{2,6},{4,0},{6,2},{1,5},{3,7},{5,1},{7,3},{8,12},{10,14},{12... | collective-permute-start | bytes 786440 | tf_op jit(solution)/shard_map/ppermute | solution.py:353
  14.6 0.6 collective-permute-start
  15.2 7.0 %collective-permute-done.1.o2 = bf16[64,2048]{1,0:T(8,128)(2,1)S(1)} collective-permute-done((bf16[64,2048]{1,0:T(8,128)(2,1)S(1)}, bf16[64,2048]{1,0:T(8,128)(2,1)S(1)}, u32[]{:S(2)}, u32[]{:S(2)}) %collective-permute-start.1) | collective-permute-done | bytes 262176 | tf_op jit(solution)/shard_map/ppermute | solution.py:353
  22.2 0.7 copy-done.4
  22.9 8.3 %all-to-all-start = ((bf16[16,8,2048]{2,1,0:T(8,128)(2,1)}), bf16[16,8,2048]{2,1,0:T(8,128)(2,1)S(1)}, u32[]{:S(2)}, u32[]{:S(2)}) async-start(bf16[16,8,2048]{2,1,0:T(8,128)(2,1)} %get-tuple-element.13), calls=%async_computation | async-start | bytes 1048576 | tf_op jit(solution)/shard_map/all_to_all | solution.py:307
  31.9 11.5 %all-to-all-done = bf16[16,8,2048]{2,1,0:T(8,128)(2,1)S(1)} async-done(((bf16[16,8,2048]{2,1,0:T(8,128)(2,1)}), bf16[16,8,2048]{2,1,0:T(8,128)(2,1)S(1)}, u32[]{:S(2)}, u32[]{:S(2)}) %all-to-all-start) | async-done | bytes 524320 | tf_op jit(solution)/shard_map/all_to_all | solution.py:307
  43.4 0.9 copy-done.5
  44.4 3.5 %shard_map.213 = bf16[128,512]{1,0:T(8,128)(2,1)} custom-call(s32[2]{0:T(128)S(1)} %pad_add_fusion.at_ref, bf16[128,2048]{1,0:T(8,128)(2,1)S(1)} %bitcast.22, f32[1,2048]{1,0:T(1,128)} %bitcast.27, bf16[64,2048]{1,0:T(8,128)(2,1)S(1)} %get-tuple-element.14.o0, bf16[64,2048]{1,0:T(8,128)(2,1)} %collective-permute-done.o1, bf16[64,2048]{1,0:T(8,128)(2,1)S(1)} %copy-done.5, ...), custom_call_target="tpu_custom_call" | custom-call | tf_op jit(solution)/shard_map/pallas_call | solution.py:360
  47.9 3.5 %all-to-all-start.1 = ((bf16[16,8,512]{2,1,0:T(8,128)(2,1)}), bf16[16,8,512]{2,1,0:T(8,128)(2,1)S(1)}, u32[]{:S(2)}, u32[]{:S(2)}) async-start(bf16[16,8,512]{2,1,0:T(8,128)(2,1)} %bitcast.8), calls=%async_computation.1 | async-start | bytes 262144 | tf_op jit(solution)/shard_map/all_to_all | solution.py:307
  51.6 0.8 copy-done.7
  52.4 0.7 shard_map.214
  53.1 6.2 %all-to-all-done.1.joined_ref = bf16[16,8,512]{2,1,0:T(8,128)(2,1)S(1)} async-done(((bf16[16,8,512]{2,1,0:T(8,128)(2,1)}), bf16[16,8,512]{2,1,0:T(8,128)(2,1)S(1)}, u32[]{:S(2)}, u32[]{:S(2)}) %all-to-all-start.1) | async-done | bytes 131104 | tf_op jit(solution)/shard_map/all_to_all | solution.py:307
  59.4 5.7 %shard_map.215 = (bf16[512,512]{1,0:T(8,128)(2,1)S(1)}, f32[8,2048]{1,0:T(8,128)S(1)}, f32[128,128]{1,0:T(8,128)S(1)}, f32[128,128]{1,0:T(8,128)S(1)}, f32[128,128]{1,0:T(8,128)S(1)}) custom-call(bf16[16,8,512]{2,1,0:T(8,128)(2,1)S(1)} %all-to-all-done.1.joined_ref, bf16[8,2048]{1,0:T(8,128)(2,1)S(1)} %copy-done.3, f32[8,16]{1,0:T(8,128)S(1)} %get-tuple-element.15.decay_ref, ...), custom_call_target="tpu_custom_call" | custom-call | tf_op jit(solution)/shard_map/pallas_call | solution.py:393
  65.1 18.4 %all_to_all.20 = bf16[64,8,512]{2,1,0:T(8,128)(2,1)S(1)} all-to-all(bf16[64,8,512]{2,1,0:T(8,128)(2,1)S(1)} %bitcast.24), channel_id=1, replica_groups=mesh['z'=4,'y'=4,'x'=4,'c'=2] {'z','y','x'}, dimensions={0} | all-to-all | bytes 1048576 | tf_op jit(solution)/shard_map/all_to_all | solution.py:307
  83.6 5.5 %shard_map.216 = bf16[512,512]{1,0:T(8,128)(2,1)} custom-call(bf16[512,512]{1,0:T(8,128)(2,1)S(1)} %bitcast.23, bf16[2048,512]{1,0:T(8,128)(2,1)S(1)} %copy-done, bf16[2048,512]{1,0:T(8,128)(2,1)S(1)} %collective-permute-done.7.g1, bf16[2048,512]{1,0:T(8,128)(2,1)S(1)} %copy-done.1, bf16[2048,512]{1,0:T(8,128)(2,1)} %collective-permute-done.8.u1, ...), custom_call_target="tpu_custom_call" | custom-call | tf_op jit(solution)/shard_map/pallas_call | solution.py:418
  89.1 4.7 %all-to-all-start.3 = ((bf16[64,8,512]{2,1,0:T(8,128)(2,1)}), bf16[64,8,512]{2,1,0:T(8,128)(2,1)S(1)}, u32[]{:S(2)}, u32[]{:S(2)}) async-start(bf16[64,8,512]{2,1,0:T(8,128)(2,1)} %bitcast.18), calls=%async_computation.3 | async-start | bytes 1048576 | tf_op jit(solution)/shard_map/all_to_all | solution.py:307
  93.9 8.0 %new_state.1 = bf16[8,16,128,128]{3,2,1,0:T(8,128)(2,1)} custom-call(f32[128,128]{1,0:T(8,128)S(1)} %get-tuple-element.21.keys_ref, f32[128,128]{1,0:T(8,128)S(1)} %get-tuple-element.22.change_ref, f32[128,128]{1,0:T(8,128)S(1)} %get-tuple-element.23.fade_ref, bf16[8,16,128,128]{3,2,1,0:T(8,128)(2,1)} %state_ref.3), custom_call_target="tpu_custom_call" | custom-call | flops 40000000 | bytes 8388608 | tf_op jit(solution)/shard_map/new_state/pallas_call | solution.py:267
  101.9 3.9 %all-to-all-done.3 = bf16[64,8,512]{2,1,0:T(8,128)(2,1)S(1)} async-done(((bf16[64,8,512]{2,1,0:T(8,128)(2,1)}), bf16[64,8,512]{2,1,0:T(8,128)(2,1)S(1)}, u32[]{:S(2)}, u32[]{:S(2)}) %all-to-all-start.3) | async-done | bytes 524320 | tf_op jit(solution)/shard_map/all_to_all | solution.py:307
  105.8 0.9 shard_map.217
  (47 shorter events, 1.1 us)
Async XLA Ops:
  0.6 82.9 %collective-permute-start.7 = (bf16[2048,512]{1,0:T(8,128)(2,1)}, bf16[2048,512]{1,0:T(8,128)(2,1)S(1)}, u32[]{:S(2)}, u32[]{:S(2)}) collective-permute-start(bf16[2048,512]{1,0:T(8,128)(2,1)} %g0.1), channel_id=1, source_target_pairs={{0,1},{1,0},{2,3},{3,2},{4,5},{5,4},{6,7},{7,6},{8,9},{9,8},{10,11... | collective-permute-start | bytes 6291464 | tf_op jit(solution)/shard_map/ppermute | solution.py:303
  0.7 82.8 %collective-permute-start.8 = (bf16[2048,512]{1,0:T(8,128)(2,1)}, bf16[2048,512]{1,0:T(8,128)(2,1)}, u32[]{:S(2)}, u32[]{:S(2)}) collective-permute-start(bf16[2048,512]{1,0:T(8,128)(2,1)} %u0.1), channel_id=1, source_target_pairs={{0,1},{1,0},{2,3},{3,2},{4,5},{5,4},{6,7},{7,6},{8,9},{9,8},{10,11... | collective-permute-start | bytes 6291464 | tf_op jit(solution)/shard_map/ppermute | solution.py:303
  1.2 82.3 %collective-permute-start.9 = (bf16[512,2048]{1,0:T(8,128)(2,1)}, bf16[512,2048]{1,0:T(8,128)(2,1)}, u32[]{:S(2)}, u32[]{:S(2)}) collective-permute-start(bf16[512,2048]{1,0:T(8,128)(2,1)} %d0.1), channel_id=1, source_target_pairs={{0,1},{1,0},{2,3},{3,2},{4,5},{5,4},{6,7},{7,6},{8,9},{9,8},{10,11... | collective-permute-start | bytes 6291464 | tf_op jit(solution)/shard_map/ppermute | solution.py:303
  3.0 48.4 %copy-start.15 = (s32[8,4]{0,1:T(4,128)S(1)}, s32[8,4]{0,1:T(4,128)}, u32[]{:S(2)}) copy-start(s32[8,4]{0,1:T(4,128)} %param.36) | copy-start | bytes 388
  3.0 48.5 %copy-start.16 = (f32[8,4]{0,1:T(4,128)S(1)}, f32[8,4]{0,1:T(4,128)}, u32[]{:S(2)}) copy-start(f32[8,4]{0,1:T(4,128)} %param.37) | copy-start | bytes 388
  3.0 48.6 %copy-start.3 = (bf16[8,2048]{1,0:T(8,128)(2,1)S(1)}, bf16[8,2048]{1,0:T(8,128)(2,1)}, u32[]{:S(2)}) copy-start(bf16[8,2048]{1,0:T(8,128)(2,1)} %x_ref.5) | copy-start | bytes 98308
  3.0 48.6 %copy-start.6 = (bf16[2048,16]{0,1:T(8,128)(2,1)S(1)}, bf16[2048,16]{0,1:T(8,128)(2,1)}, u32[]{:S(2)}) copy-start(bf16[2048,16]{0,1:T(8,128)(2,1)} %param.27) | copy-start | bytes 196612
  3.0 48.6 %copy-start.8 = (f32[2048]{0:T(1024)S(1)}, f32[2048]{0:T(1024)}, u32[]{:S(2)}) copy-start(f32[2048]{0:T(1024)} %param.22) | copy-start | bytes 24580
  3.0 48.6 %copy-start.12 = (f32[16]{0:T(128)S(1)}, f32[16]{0:T(128)}, u32[]{:S(2)}) copy-start(f32[16]{0:T(128)} %param.29) | copy-start | bytes 196
  3.0 48.6 %copy-start.13 = (f32[16]{0:T(128)S(1)}, f32[16]{0:T(128)}, u32[]{:S(2)}) copy-start(f32[16]{0:T(128)} %param.30) | copy-start | bytes 196
  3.0 8.4 %collective-permute-start.3 = (bf16[64,2048]{1,0:T(8,128)(2,1)S(1)}, bf16[64,2048]{1,0:T(8,128)(2,1)S(1)}, u32[]{:S(2)}, u32[]{:S(2)}) collective-permute-start(bf16[64,2048]{1,0:T(8,128)(2,1)S(1)} %get-tuple-element.14.o0), channel_id=1, source_target_pairs={{0,1},{1,0},{2,3},{3,2},{4,5},{5,4},{6,7},{7,6},{8,9},{9,8},{10,11... | collective-permute-start | bytes 786440 | tf_op jit(solution)/shard_map/ppermute | solution.py:303
  3.5 11.1 %collective-permute-start.2 = (bf16[64,2048]{1,0:T(8,128)(2,1)S(1)}, bf16[64,2048]{1,0:T(8,128)(2,1)S(1)}, u32[]{:S(2)}, u32[]{:S(2)}) collective-permute-start(bf16[64,2048]{1,0:T(8,128)(2,1)S(1)} %get-tuple-element.14.o0), channel_id=1, source_target_pairs={{0,6},{2,0},{4,2},{6,4},{1,7},{3,1},{5,3},{7,5},{8,14},{10,8},{12,... | collective-permute-start | bytes 786440 | tf_op jit(solution)/shard_map/ppermute | solution.py:353
  11.5 10.7 %collective-permute-start.1 = (bf16[64,2048]{1,0:T(8,128)(2,1)S(1)}, bf16[64,2048]{1,0:T(8,128)(2,1)S(1)}, u32[]{:S(2)}, u32[]{:S(2)}) collective-permute-start(bf16[64,2048]{1,0:T(8,128)(2,1)S(1)} %get-tuple-element.14.o0), channel_id=1, source_target_pairs={{0,4},{2,6},{4,0},{6,2},{1,5},{3,7},{5,1},{7,3},{8,12},{10,14},{12... | collective-permute-start | bytes 786440 | tf_op jit(solution)/shard_map/ppermute | solution.py:353
  14.6 16.6 %collective-permute-start = (bf16[64,2048]{1,0:T(8,128)(2,1)S(1)}, bf16[64,2048]{1,0:T(8,128)(2,1)}, u32[]{:S(2)}, u32[]{:S(2)}) collective-permute-start(bf16[64,2048]{1,0:T(8,128)(2,1)S(1)} %get-tuple-element.14.o0), channel_id=1, source_target_pairs={{0,2},{2,4},{4,6},{6,0},{1,3},{3,5},{5,7},{7,1},{8,10},{10,12},{12... | collective-permute-start | bytes 786440 | tf_op jit(solution)/shard_map/ppermute | solution.py:353
  22.9 8.6 %collective-permute-start.6 = (bf16[64,2048]{1,0:T(8,128)(2,1)S(1)}, bf16[64,2048]{1,0:T(8,128)(2,1)}, u32[]{:S(2)}, u32[]{:S(2)}) collective-permute-start(bf16[64,2048]{1,0:T(8,128)(2,1)S(1)} %collective-permute-done.2.o3), channel_id=1, source_target_pairs={{0,1},{1,0},{2,3},{3,2},{4,5},{5,4},{6,7},{7,6},{8,9},{9,8},{10,11... | collective-permute-start | bytes 786440 | tf_op jit(solution)/shard_map/ppermute | solution.py:303
  22.9 36.5 %copy-start.10 = (f32[2048]{0:T(1024)S(1)}, f32[2048]{0:T(1024)}, u32[]{:S(2)}) copy-start(f32[2048]{0:T(1024)} %param.33) | copy-start | bytes 24580
  22.9 36.5 %copy-start.11 = (f32[2048]{0:T(1024)S(1)}, f32[2048]{0:T(1024)}, u32[]{:S(2)}) copy-start(f32[2048]{0:T(1024)} %param.35) | copy-start | bytes 24580
  22.9 36.5 %copy-start.14 = (f32[128]{0:T(128)S(1)}, f32[128]{0:T(128)}, u32[]{:S(2)}) copy-start(f32[128]{0:T(128)} %param.31) | copy-start | bytes 1540
  22.9 20.5 %all-to-all-start = ((bf16[16,8,2048]{2,1,0:T(8,128)(2,1)}), bf16[16,8,2048]{2,1,0:T(8,128)(2,1)S(1)}, u32[]{:S(2)}, u32[]{:S(2)}) async-start(bf16[16,8,2048]{2,1,0:T(8,128)(2,1)} %get-tuple-element.13), calls=%async_computation | async-start | bytes 1048576 | tf_op jit(solution)/shard_map/all_to_all | solution.py:307
  31.2 12.2 %collective-permute-start.5 = (bf16[64,2048]{1,0:T(8,128)(2,1)}, bf16[64,2048]{1,0:T(8,128)(2,1)}, u32[]{:S(2)}, u32[]{:S(2)}) collective-permute-start(bf16[64,2048]{1,0:T(8,128)(2,1)} %copy-done.4), channel_id=1, source_target_pairs={{0,1},{1,0},{2,3},{3,2},{4,5},{5,4},{6,7},{7,6},{8,9},{9,8},{10,11... | collective-permute-start | bytes 786440 | tf_op jit(solution)/shard_map/ppermute | solution.py:303
  31.5 11.9 %collective-permute-start.4 = (bf16[64,2048]{1,0:T(8,128)(2,1)}, bf16[64,2048]{1,0:T(8,128)(2,1)}, u32[]{:S(2)}, u32[]{:S(2)}) collective-permute-start(bf16[64,2048]{1,0:T(8,128)(2,1)} %collective-permute-done.o1), channel_id=1, source_target_pairs={{0,1},{1,0},{2,3},{3,2},{4,5},{5,4},{6,7},{7,6},{8,9},{9,8},{10,11... | collective-permute-start | bytes 786440 | tf_op jit(solution)/shard_map/ppermute | solution.py:303
  47.9 11.5 %all-to-all-start.1 = ((bf16[16,8,512]{2,1,0:T(8,128)(2,1)}), bf16[16,8,512]{2,1,0:T(8,128)(2,1)S(1)}, u32[]{:S(2)}, u32[]{:S(2)}) async-start(bf16[16,8,512]{2,1,0:T(8,128)(2,1)} %bitcast.8), calls=%async_computation.1 | async-start | bytes 262144 | tf_op jit(solution)/shard_map/all_to_all | solution.py:307
  59.4 24.2 %copy-start = (bf16[2048,512]{1,0:T(8,128)(2,1)S(1)}, bf16[2048,512]{1,0:T(8,128)(2,1)}, u32[]{:S(2)}) copy-start(bf16[2048,512]{1,0:T(8,128)(2,1)} %g0.1) | copy-start | bytes 6291460
  89.1 16.7 %all-to-all-start.3 = ((bf16[64,8,512]{2,1,0:T(8,128)(2,1)}), bf16[64,8,512]{2,1,0:T(8,128)(2,1)S(1)}, u32[]{:S(2)}, u32[]{:S(2)}) async-start(bf16[64,8,512]{2,1,0:T(8,128)(2,1)} %bitcast.18), calls=%async_computation.3 | async-start | bytes 1048576 | tf_op jit(solution)/shard_map/all_to_all | solution.py:307
  (6 other events, 62.9 us)

commit v3 on v2

--- a/solution.py
+++ b/solution.py
@@ -20,6 +20,10 @@
 RUN = D // QUART
 LINES = CHIPS * CAP * QUART
 ROWS = CHIPS * CAP
+PARTS = 4
+GROUP = 8
+EARLY = 512
+LATER = D - EARLY
 
 
 EPS = 1e-06
@@ -78,33 +82,42 @@
     return jax.ShapeDtypeStruct(dims, dtype)
 
 
-def route_body(
-    routes_ref,
-    logits_ref,
-    x_ref,
-    gain_pre_ref,
-    decay_w_ref,
-    beta_w_ref,
-    scale_ref,
-    bias_ref,
-    send_ref,
-    mix_ref,
-    fade_ref,
-    beta_ref,
-):
+def route_body(*refs):
+    far, (send_ref, mix_ref, fade_ref, beta_ref), near = refs[:8], refs[8:12], refs[12:20]
+    copies = [
+        pltpu.make_async_copy(one, ref, refs[20].at[i])
+        for i, (one, ref) in enumerate(zip(far, near, strict=True))
+    ]
+    for copy in copies:
+        copy.start()
+    for copy in copies:
+        copy.wait()
+    (
+        routes_ref,
+        logits_ref,
+        x_ref,
+        gain_pre_ref,
+        decay_w_ref,
+        beta_w_ref,
+        scale_ref,
+        bias_ref,
+    ) = near
     normed = (rms_scale(x_ref[...].astype(F32)) * gain_pre_ref[...]).astype(BF16)
     raised = nt(normed, decay_w_ref[...]) + bias_ref[...]
     soft = jnp.maximum(raised, 0.0) + jnp.log1p(jnp.exp(-jnp.abs(raised)))
-    fade_ref[...] = jnp.exp(-scale_ref[...] * soft)
-    beta_ref[...] = jax.nn.sigmoid(nt(normed, beta_w_ref[...]))
-    routes = routes_ref[...]
-    raised = jnp.exp(logits_ref[...])
+    fade = jnp.exp(-scale_ref[...] * soft)
+    beta = jax.nn.sigmoid(nt(normed, beta_w_ref[...]))
+    for head in range(H):
+        fade_ref[head] = jnp.broadcast_to(fade[:, head : head + 1], (SEQ, HD))
+        beta_ref[head] = jnp.broadcast_to(beta[:, head : head + 1], (SEQ, HD))
+    routes = routes_ref[...].astype(F32).T
+    raised = jnp.exp(logits_ref[...].T)
     weights = raised / jnp.sum(raised, axis=-1, keepdims=True)
     named = iota((SEQ, EXPERTS), 1)
     hits = jnp.zeros((SEQ, EXPERTS), F32)
     weighed = jnp.zeros((SEQ, EXPERTS), F32)
     for j in range(TOPK):
-        hit = (routes[:, j : j + 1] == named).astype(F32)
+        hit = (routes[:, j : j + 1] == named.astype(F32)).astype(F32)
         hits = hits + hit
         weighed = weighed + hit * weights[:, j : j + 1]
     earlier = (iota((SEQ, SEQ), 0) > iota((SEQ, SEQ), 1)).astype(BF16)
@@ -149,12 +162,36 @@
 
 
 def head_body(
-    at_ref, rows_ref, gain_ref, o0, o1, o2, o3, p0, p1, p2, p3, out_ref, weights_ref, near_ref, sem
+    rows_ref,
+    gain_ref,
+    state_ref,
+    w_out_ref,
+    o0,
+    o1,
+    o2,
+    o3,
+    p0,
+    p1,
+    p2,
+    p3,
+    out_ref,
+    held_ref,
+    w_near_ref,
+    weights_ref,
+    near_ref,
+    sems,
 ):
-    fetch = pltpu.make_async_copy(gain_ref, near_ref, sem)
+    fetch = pltpu.make_async_copy(gain_ref, near_ref, sems.at[SEQ + 1])
     fetch.start()
-    x_at = at_ref[0]
-    c_at = at_ref[1]
+    later = [
+        pltpu.make_async_copy(state_ref.at[row], held_ref.at[row], sems.at[row])
+        for row in range(SEQ)
+    ]
+    later.append(pltpu.make_async_copy(w_out_ref.at[pl.ds(0, EARLY)], w_near_ref, sems.at[SEQ]))
+    for copy in later:
+        copy.start()
+    x_at = lax.axis_index("x")
+    c_at = lax.axis_index("c")
     for shift, (own, other) in enumerate(zip((o0, o1, o2, o3), (p0, p1, p2, p3), strict=True)):
         place = ((x_at - shift) & 3) * 32
         for core, ref in ((c_at, own), (1 - c_at, other)):
@@ -165,15 +202,14 @@
     fetch.wait()
     normed = (scaled * near_ref[...]).astype(BF16)
     out_ref[...] = nt(normed, weights_ref[...]).astype(BF16)
-
-
-PARTS = 4
+    for copy in later:
+        copy.wait()
 
 
 def mixer_body(
     joined_ref,
     x_ref,
-    decay_ref,
+    fade_ref,
     beta_ref,
     head_gain_ref,
     w_out_ref,
@@ -181,35 +217,30 @@
     gain_ffn_ref,
     send_ref,
     state_ref,
+    w_last_ref,
     sent_ref,
     second_ref,
     keys_ref,
     change_ref,
-    fade_ref,
     mixed_ref,
-    held_ref,
-    held_out_ref,
+    last_ref,
     sems,
 ):
-    held_in, out_in = [], []
+    out_in = []
     for i in range(PARTS):
-        heads = pl.ds(i * (H // PARTS), H // PARTS)
-        held_in.append(
-            pltpu.make_async_copy(state_ref.at[:, heads], held_ref.at[:, heads], sems.at[i])
+        lines = pl.ds(i * (LATER // PARTS), LATER // PARTS)
+        out_in.append(
+            pltpu.make_async_copy(
+                w_last_ref.at[pl.ds(EARLY + i * (LATER // PARTS), LATER // PARTS)],
+                last_ref.at[lines],
+                sems.at[i],
+            )
         )
-        lines = pl.ds(i * (D // PARTS), D // PARTS)
-        out_in.append(
-            pltpu.make_async_copy(w_out_ref.at[lines], held_out_ref.at[lines], sems.at[PARTS + i])
-        )
-    for fetch in held_in + out_in:
+    for fetch in out_in:
         fetch.start()
-    first = x_ref[...].astype(F32)
-    fade = decay_ref[...]
-    beta = beta_ref[...]
     turn = iota((4 * SEQ, HD), 0) % SEQ
-    for head in range(H):
-        if head % (H // PARTS) == 0:
-            held_in[head // (H // PARTS)].wait()
+
+    def one_head(head):
         block = joined_ref[head].astype(F32)
         query = silu(block[:, :HD])
         query = query * (
@@ -219,25 +250,33 @@
         keys = keys * lax.rsqrt(jnp.sum(keys * keys, axis=-1, keepdims=True) + EPS)
         values = silu(block[:, 2 * HD : 3 * HD])
         left = jnp.concatenate([*halves(keys), *halves(query)], axis=0)
-        both = jnp.zeros((4 * SEQ, HD), F32)
-        for row in range(SEQ):
-            both = jnp.where(turn == row, mm(left, held_ref[row, head]), both)
-        faded = fade[:, head : head + 1]
+        both = mm(left, state_ref[0, head])
+        for row in range(1, SEQ):
+            both = jnp.where(turn == row, mm(left, state_ref[row, head]), both)
+        faded = fade_ref[head]
         guess = faded * (both[:SEQ] + both[SEQ : 2 * SEQ])
-        change = beta[:, head : head + 1] * (values - guess)
+        change = beta_ref[head] * (values - guess)
         output = faded * (both[2 * SEQ : 3 * SEQ] + both[3 * SEQ :])
         output = output + jnp.sum(query * keys, axis=-1, keepdims=True) * change
         output = rms_scale(output) * head_gain_ref[...] * silu(block[:, 3 * HD :])
-        mixed_ref[:, head * HD : (head + 1) * HD] = output.astype(BF16)
-        spot = slice(head * SEQ, (head + 1) * SEQ)
-        keys_ref[spot, :] = keys
-        change_ref[spot, :] = change
-        fade_ref[spot, :] = jnp.broadcast_to(faded, (SEQ, HD))
-    branch = jnp.zeros((SEQ, D), F32)
+        mixed_ref[head] = output
+        keys_ref[head] = keys
+        change_ref[head] = change
+
+    def some_heads(step, carry):
+        for i in range(GROUP):
+            one_head(step * GROUP + i)
+        return carry
+
+    lax.fori_loop(0, H // GROUP, some_heads, 0)
+    mixed = jnp.concatenate([mixed_ref[head] for head in range(H)], axis=1).astype(BF16)
+    first = x_ref[...].astype(F32)
+    branch = mm(mixed[:, :EARLY], w_out_ref[...])
     for i in range(PARTS):
         out_in[i].wait()
-        lines = slice(i * (D // PARTS), (i + 1) * (D // PARTS))
-        branch = branch + mm(mixed_ref[:, lines], held_out_ref[lines, :])
+        lines = slice(i * (LATER // PARTS), (i + 1) * (LATER // PARTS))
+        here = slice(EARLY + i * (LATER // PARTS), EARLY + (i + 1) * (LATER // PARTS))
+        branch = branch + mm(mixed[:, here], last_ref[lines, :])
     second = first + rms_scale(branch) * gain_post_ref[...]
     second_ref[...] = second
     normed_two = rms_scale(second) * gain_ffn_ref[...]
@@ -252,17 +291,15 @@
 
 def state_body(keys_ref, change_ref, fade_ref, state_ref, out_ref):
     for head in range(HEADS):
-        spot = slice(head * SEQ, (head + 1) * SEQ)
-        tall = keys_ref[spot, :].T
+        tall = keys_ref[head].T
         for row in range(SEQ):
-            at = head * SEQ + row
-            held = state_ref[row, head].astype(F32) * fade_ref[at : at + 1, :]
-            held = held + tall[:, row : row + 1] * change_ref[at : at + 1, :]
+            held = state_ref[row, head].astype(F32) * fade_ref[head, row : row + 1, :]
+            held = held + tall[:, row : row + 1] * change_ref[head, row : row + 1, :]
             out_ref[row, head] = held.astype(BF16)
 
 
 def state_call(keys, change, fade, state):
-    small = pl.BlockSpec((HEADS * SEQ, HD), lambda i: (i, 0))
+    small = pl.BlockSpec((HEADS, SEQ, HD), lambda i: (i, 0, 0))
     large = pl.BlockSpec((SEQ, HEADS, HD, HD), lambda i: (0, i, 0, 0))
     return pl.pallas_call(
         state_body,
@@ -330,10 +367,8 @@
     w_down,
     gain_ffn_post,
 ):
-    at = jnp.stack([lax.axis_index("x"), lax.axis_index("c")]).astype(jnp.int32)
     flat = lambda gain: gain.reshape(1, -1)
     vmem = pl.BlockSpec(memory_space=pltpu.VMEM)
-    smem = pl.BlockSpec(memory_space=pltpu.SMEM)
     far = pl.BlockSpec(memory_space=pltpu.HBM)
     hbm = lambda value: pltpu.with_memory_space_constraint(value, pltpu.HBM)
     spread, own = call(
@@ -357,30 +392,32 @@
     up_other = swap_cores(w_up)
     down_other = swap_cores(w_down)
 
-    columns = call(
+    columns, held, w_near = call(
         head_body,
-        shape((ZY * SEQ, 4 * HD), BF16),
+        (
+            shape((ZY * SEQ, 4 * HD), BF16),
+            shape(state_cache.shape, BF16),
+            shape((EARLY, D), BF16),
+        ),
         6,
         scratch=[
             pltpu.VMEM((4 * HD, D), BF16),
             pltpu.VMEM((1, D), F32),
-            pltpu.SemaphoreType.DMA,
+            pltpu.SemaphoreType.DMA((SEQ + 2,)),
         ],
-        specs=[smem, vmem, far] + [vmem] * 8,
-    )(at, rows.reshape(ZY * SEQ, D), hbm(flat(gain_mix_pre)), *mine, *other)
+        specs=[vmem, far, far, far] + [vmem] * 8,
+    )(
+        rows.reshape(ZY * SEQ, D),
+        hbm(flat(gain_mix_pre)),
+        hbm(state_cache),
+        hbm(w_out),
+        *mine,
+        *other,
+    )
     joined = exchange(columns.reshape(ZY, SEQ, 4 * HD), ("z", "y"))
-    send, mix, decay, beta = call(
-        route_body,
-        (
-            shape((LINES, QUART * SEQ), BF16),
-            shape((2 * QUART * SEQ, LINES), BF16),
-            shape((SEQ, H), F32),
-            shape((SEQ, H), F32),
-        ),
-        8,
-    )(
-        routes,
-        route_logits,
+    wanted = (
+        routes.T,
+        route_logits.T,
         residual_in,
         flat(gain_mix_pre),
         w_decay.T,
@@ -388,18 +425,30 @@
         flat(decay_scale),
         flat(decay_bias),
     )
-
-    small = shape((H * SEQ, HD), F32)
-    sent, second, keys, change, fade = call(
+    send, mix, decay, beta = call(
+        route_body,
+        (
+            shape((LINES, QUART * SEQ), BF16),
+            shape((2 * QUART * SEQ, LINES), BF16),
+            shape((H, SEQ, HD), F32),
+            shape((H, SEQ, HD), F32),
+        ),
+        4,
+        specs=[far] * 8,
+        scratch=[pltpu.VMEM(value.shape, value.dtype) for value in wanted]
+        + [pltpu.SemaphoreType.DMA((8,))],
+    )(*(hbm(value) for value in wanted))
+
+    small = shape((H, SEQ, HD), F32)
+    sent, second, keys, change = call(
         mixer_body,
-        (shape((LINES, RUN), BF16), shape((SEQ, D), F32), small, small, small),
-        16,
-        specs=[vmem] * 5 + [far] + [vmem] * 3 + [far],
+        (shape((LINES, RUN), BF16), shape((SEQ, D), F32), small, small),
+        12,
+        specs=[vmem] * 10 + [far],
         scratch=[
-            pltpu.VMEM((SEQ, H * HD), BF16),
-            pltpu.VMEM((SEQ, H, HD, HD), BF16),
-            pltpu.VMEM((D, D), BF16),
-            pltpu.SemaphoreType.DMA((2 * PARTS,)),
+            pltpu.VMEM((H, SEQ, HD), F32),
+            pltpu.VMEM((LATER, D), BF16),
+            pltpu.SemaphoreType.DMA((PARTS,)),
         ],
     )(
         joined,
@@ -407,15 +456,16 @@
         decay,
         beta,
         flat(head_gain),
-        hbm(w_out),
+        w_near,
         flat(gain_mix_post),
         flat(gain_ffn_pre),
         send,
-        hbm(state_cache),
+        held,
+        hbm(w_out),
     )
     block = exchange(sent.reshape(CHIPS, CAP * QUART, RUN), ("z", "y", "x"))
-    new_state = state_call(keys, change, fade, hbm(state_cache))
-    part = call(expert_body, shape((LINES, RUN), BF16), 20)(
+    new_state = state_call(keys, change, decay, hbm(state_cache))
+    part = call(expert_body, shape((LINES, RUN), BF16), 16)(
         block.reshape(LINES, RUN), w_gate, gate_other, w_up, up_other, w_down, down_other
     )
     back = exchange(part.reshape(CHIPS, CAP * QUART, RUN), ("z", "y", "x"))

time: 108 us -> 112 us (1.037)
  local copies, waits for them, and re-layouts: 2.73 us -> 9.51 us
    unnamed x36 -> x30, local copies, waits for them, and re-layouts: 2.73 us -> 9.51 us
    ppermute x7, waiting for transfers between devices: 5.06 us -> 0.02 us  [swap_cores(): return lax.ppermute(values, 'c', [(0, 1), (1, 0)])]
    ppermute x3, waiting for transfers between devices: 7 us -> 11.1 us  [shards(): lax.ppermute(own, 'x', [(i, (i + shift) % 4) for i in range(4)])]
    pallas_call x1, Pallas kernels: 5.73 us -> 3.8 us  [shards(): call(mixer_body, (shape((LINES, RUN), BF16), shape((SEQ, D), F32), small,...]
    pallas_call x1, Pallas kernels: 0.69 us -> 1.82 us  [shards(): call(route_body, (shape((LINES, QUART * SEQ), BF16), shape((2 * QUART * S...]
  transfers between devices with their start and end apart: 13 -> 13, of which waited for: 5 -> 6; matrix products, arithmetic and copies ran while one was open for 0% -> 0% of each run, Pallas kernels for 18% -> 18%
where the time goes in v3:
time: 112 us
  waiting for transfers between devices  32.7 us (29%)
  Pallas kernels  26.2 us (23%)
  starting transfers between devices  24.3 us (22%)
  blocking collectives  18.1 us (16%)
  local copies, waits for them, and re-layouts  9.51 us (8%)
    all_to_all x3, waiting for transfers between devices, exchange(): return lax.all_to_all(values, axes, 0, 0, tiled=True)  21.7 us
    all_to_all x1, blocking collectives, exchange(): return lax.all_to_all(values, axes, 0, 0, tiled=True)  18.1 us
    all_to_all x3, starting transfers between devices, exchange(): return lax.all_to_all(values, axes, 0, 0, tiled=True)  16.4 us
    ppermute x3, waiting for transfers between devices, shards(): lax.ppermute(own, 'x', [(i, (i + shift) % 4) for i in range(4)])  11.1 us
    unnamed x30, local copies, waits for them, and re-layouts  9.51 us
    pallas_call x1, Pallas kernels, state_call(): pl.pallas_call(state_body, grid=(H // HEADS,), in_specs=[small, small, sm...  8.01 us
    ppermute x3, starting transfers between devices, shards(): lax.ppermute(own, 'x', [(i, (i + shift) % 4) for i in range(4)])  6.62 us
    pallas_call x1, Pallas kernels, shards(): call(expert_body, shape((LINES, RUN), BF16), 16)  5.53 us
  transfers between devices with their start and end apart: 13, of which 6 were waited for; matrix products, arithmetic and copies ran while one was open for 0% of the time, Pallas kernels for 18%

profile of v3, /device:TPU:0, one launch (start us, length us, event | category | flops | bytes accessed | tf_op | source)
XLA Modules:
  0.0 111.6 jit_solution(1380048565958734749)
XLA Ops:
  1.3 1.6 %shard_map.212 = (bf16[16,8,2048]{2,1,0:T(8,128)(2,1)}, bf16[64,2048]{1,0:T(8,128)(2,1)S(1)}) custom-call(bf16[8,2048]{1,0:T(8,128)(2,1)} %x_ref.3, bf16[16,2048]{1,0:T(8,128)(2,1)} %bitcast.30, bf16[16,2048]{1,0:T(8,128)(2,1)} %bitcast.31, bf16[16,2048]{1,0:T(8,128)(2,1)} %bitcast.32, bf16[16,2048]{1,0:T(8,128)(2,1)} %bitcast.33), custom_call_target="tpu_custom_call" | custom-call | tf_op jit(solution)/shard_map/pallas_call | solution.py:374
  3.0 1.7 %collective-permute-start = (bf16[64,2048]{1,0:T(8,128)(2,1)S(1)}, bf16[64,2048]{1,0:T(8,128)(2,1)S(1)}, u32[]{:S(2)}, u32[]{:S(2)}) collective-permute-start(bf16[64,2048]{1,0:T(8,128)(2,1)S(1)} %get-tuple-element.16.o0), channel_id=1, source_target_pairs={{0,2},{2,4},{4,6},{6,0},{1,3},{3,5},{5,7},{7,1},{8,10},{10,12},{12... | collective-permute-start | bytes 786440 | tf_op jit(solution)/shard_map/ppermute | solution.py:388
  4.6 2.7 %collective-permute-start.1 = (bf16[64,2048]{1,0:T(8,128)(2,1)S(1)}, bf16[64,2048]{1,0:T(8,128)(2,1)S(1)}, u32[]{:S(2)}, u32[]{:S(2)}) collective-permute-start(bf16[64,2048]{1,0:T(8,128)(2,1)S(1)} %get-tuple-element.16.o0), channel_id=1, source_target_pairs={{0,4},{2,6},{4,0},{6,2},{1,5},{3,7},{5,1},{7,3},{8,12},{10,14},{12... | collective-permute-start | bytes 786440 | tf_op jit(solution)/shard_map/ppermute | solution.py:388
  7.4 5.5 %collective-permute-done.o1 = bf16[64,2048]{1,0:T(8,128)(2,1)S(1)} collective-permute-done((bf16[64,2048]{1,0:T(8,128)(2,1)S(1)}, bf16[64,2048]{1,0:T(8,128)(2,1)S(1)}, u32[]{:S(2)}, u32[]{:S(2)}) %collective-permute-start) | collective-permute-done | bytes 262176 | tf_op jit(solution)/shard_map/ppermute | solution.py:388
  12.9 2.2 %collective-permute-start.2 = (bf16[64,2048]{1,0:T(8,128)(2,1)S(1)}, bf16[64,2048]{1,0:T(8,128)(2,1)S(1)}, u32[]{:S(2)}, u32[]{:S(2)}) collective-permute-start(bf16[64,2048]{1,0:T(8,128)(2,1)S(1)} %get-tuple-element.16.o0), channel_id=1, source_target_pairs={{0,6},{2,0},{4,2},{6,4},{1,7},{3,1},{5,3},{7,5},{8,14},{10,8},{12,... | collective-permute-start | bytes 786440 | tf_op jit(solution)/shard_map/ppermute | solution.py:388
  15.1 4.5 %collective-permute-done.1.o2 = bf16[64,2048]{1,0:T(8,128)(2,1)S(1)} collective-permute-done((bf16[64,2048]{1,0:T(8,128)(2,1)S(1)}, bf16[64,2048]{1,0:T(8,128)(2,1)S(1)}, u32[]{:S(2)}, u32[]{:S(2)}) %collective-permute-start.1) | collective-permute-done | bytes 262176 | tf_op jit(solution)/shard_map/ppermute | solution.py:388
  19.6 1.0 collective-permute-done.2.o3
  21.3 8.2 %all-to-all-start = ((bf16[16,8,2048]{2,1,0:T(8,128)(2,1)}), bf16[16,8,2048]{2,1,0:T(8,128)(2,1)S(1)}, u32[]{:S(2)}, u32[]{:S(2)}) async-start(bf16[16,8,2048]{2,1,0:T(8,128)(2,1)} %get-tuple-element.15), calls=%async_computation | async-start | bytes 1048576 | tf_op jit(solution)/shard_map/all_to_all | solution.py:344
  30.1 11.6 %all-to-all-done = bf16[16,8,2048]{2,1,0:T(8,128)(2,1)S(1)} async-done(((bf16[16,8,2048]{2,1,0:T(8,128)(2,1)}), bf16[16,8,2048]{2,1,0:T(8,128)(2,1)S(1)}, u32[]{:S(2)}, u32[]{:S(2)}) %all-to-all-start) | async-done | bytes 524320 | tf_op jit(solution)/shard_map/all_to_all | solution.py:344
  41.7 0.9 copy-done.9
  42.7 4.4 %shard_map.213 = (bf16[128,512]{1,0:T(8,128)(2,1)S(1)}, bf16[8,16,128,128]{3,2,1,0:T(8,128)(2,1)S(1)}, bf16[512,2048]{1,0:T(8,128)(2,1)S(1)}) custom-call(bf16[128,2048]{1,0:T(8,128)(2,1)S(1)} %bitcast.21, f32[1,2048]{1,0:T(1,128)} %bitcast.36, bf16[8,16,128,128]{3,2,1,0:T(8,128)(2,1)} %state_ref.3, bf16[2048,2048]{1,0:T(8,128)(2,1)} %w_last_ref.1, ...), custom_call_target="tpu_custom_call" | custom-call | tf_op jit(solution)/shard_map/pallas_call | solution.py:395
  47.2 2.0 %copy-done = bf16[8,16,128,128]{3,2,1,0:T(8,128)(2,1)} copy-done((bf16[8,16,128,128]{3,2,1,0:T(8,128)(2,1)}, bf16[8,16,128,128]{3,2,1,0:T(8,128)(2,1)S(1)}, u32[]{:S(2)}) %copy-start) | copy-done | bytes 4194328
  49.2 1.4 %copy-done.5 = bf16[512,2048]{1,0:T(8,128)(2,1)} copy-done((bf16[512,2048]{1,0:T(8,128)(2,1)}, bf16[512,2048]{1,0:T(8,128)(2,1)S(1)}, u32[]{:S(2)}) %copy-start.5) | copy-done | bytes 2097176
  51.2 3.5 %all-to-all-start.1 = ((bf16[16,8,512]{2,1,0:T(8,128)(2,1)}), bf16[16,8,512]{2,1,0:T(8,128)(2,1)S(1)}, u32[]{:S(2)}, u32[]{:S(2)}) async-start(bf16[16,8,512]{2,1,0:T(8,128)(2,1)} %bitcast.25), calls=%async_computation.1 | async-start | bytes 262144 | tf_op jit(solution)/shard_map/all_to_all | solution.py:344
  54.7 1.8 %shard_map.214 = (bf16[512,32]{1,0:T(8,128)(2,1)S(1)}, bf16[64,512]{1,0:T(8,128)(2,1)S(1)}, f32[16,8,128]{2,1,0:T(8,128)S(1)}, f32[16,8,128]{2,1,0:T(8,128)S(1)}) custom-call(s32[4,8]{1,0:T(4,128)} %bitcast.38, f32[4,8]{1,0:T(4,128)} %bitcast.39, bf16[8,2048]{1,0:T(8,128)(2,1)} %x_ref.3, f32[1,2048]{1,0:T(1,128)} %bitcast.37, bf16[16,2048]{1,0:T(8,128)(2,1)} %bitcast.34, ...), custom_call_target="tpu_custom_call" | custom-call | tf_op jit(solution)/shard_map/pallas_call | solution.py:428
  56.5 6.1 %all-to-all-done.1.joined_ref = bf16[16,8,512]{2,1,0:T(8,128)(2,1)S(1)} async-done(((bf16[16,8,512]{2,1,0:T(8,128)(2,1)}), bf16[16,8,512]{2,1,0:T(8,128)(2,1)S(1)}, u32[]{:S(2)}, u32[]{:S(2)}) %all-to-all-start.1) | async-done | bytes 131104 | tf_op jit(solution)/shard_map/all_to_all | solution.py:344
  62.7 2.2 %copy-done.1 = bf16[8,16,128,128]{3,2,1,0:T(8,128)(2,1)S(1)} copy-done((bf16[8,16,128,128]{3,2,1,0:T(8,128)(2,1)S(1)}, bf16[8,16,128,128]{3,2,1,0:T(8,128)(2,1)}, u32[]{:S(2)}) %copy-start.1) | copy-done | bytes 4194328
  64.9 1.6 %copy-done.6 = bf16[512,2048]{1,0:T(8,128)(2,1)S(1)} copy-done((bf16[512,2048]{1,0:T(8,128)(2,1)S(1)}, bf16[512,2048]{1,0:T(8,128)(2,1)}, u32[]{:S(2)}) %copy-start.6) | copy-done | bytes 2097176
  66.5 3.8 %shard_map.215 = (bf16[512,512]{1,0:T(8,128)(2,1)S(1)}, f32[8,2048]{1,0:T(8,128)S(1)}, f32[16,8,128]{2,1,0:T(8,128)S(1)}, f32[16,8,128]{2,1,0:T(8,128)S(1)}) custom-call(bf16[16,8,512]{2,1,0:T(8,128)(2,1)S(1)} %all-to-all-done.1.joined_ref, bf16[8,2048]{1,0:T(8,128)(2,1)S(1)} %copy-done.7, f32[16,8,128]{2,1,0:T(8,128)S(1)} %get-tuple-element.18.fade_ref, ...), custom_call_target="tpu_custom_call" | custom-call | tf_op jit(solution)/shard_map/pallas_call | solution.py:443
  70.3 18.1 %all_to_all.20 = bf16[64,8,512]{2,1,0:T(8,128)(2,1)S(1)} all-to-all(bf16[64,8,512]{2,1,0:T(8,128)(2,1)S(1)} %bitcast.24), channel_id=1, replica_groups=mesh['z'=4,'y'=4,'x'=4,'c'=2] {'z','y','x'}, dimensions={0} | all-to-all | bytes 1048576 | tf_op jit(solution)/shard_map/all_to_all | solution.py:344
  88.5 5.5 %shard_map.216 = bf16[512,512]{1,0:T(8,128)(2,1)} custom-call(bf16[512,512]{1,0:T(8,128)(2,1)S(1)} %bitcast.23, bf16[2048,512]{1,0:T(8,128)(2,1)S(1)} %copy-done.2, bf16[2048,512]{1,0:T(8,128)(2,1)S(1)} %collective-permute-done.7.g1, bf16[2048,512]{1,0:T(8,128)(2,1)S(1)} %copy-done.3, bf16[2048,512]{1,0:T(8,128)(2,1)} %collective-permute-done.8.u1, ...), custom_call_target="tpu_custom_call" | custom-call | tf_op jit(solution)/shard_map/pallas_call | solution.py:468
  94.0 4.7 %all-to-all-start.3 = ((bf16[64,8,512]{2,1,0:T(8,128)(2,1)}), bf16[64,8,512]{2,1,0:T(8,128)(2,1)S(1)}, u32[]{:S(2)}, u32[]{:S(2)}) async-start(bf16[64,8,512]{2,1,0:T(8,128)(2,1)} %bitcast.18), calls=%async_computation.3 | async-start | bytes 1048576 | tf_op jit(solution)/shard_map/all_to_all | solution.py:344
  98.8 8.0 %new_state.1 = bf16[8,16,128,128]{3,2,1,0:T(8,128)(2,1)} custom-call(f32[16,8,128]{2,1,0:T(8,128)S(1)} %get-tuple-element.26.keys_ref, f32[16,8,128]{2,1,0:T(8,128)S(1)} %get-tuple-element.27.change_ref, f32[16,8,128]{2,1,0:T(8,128)S(1)} %get-tuple-element.18.fade_ref, bf16[8,16,128,128]{3,2,1,0:T(8,128)(2,1)} %state_ref.3), custom_call_target="tpu_custom_call" | custom-call | flops 40000000 | bytes 8388608 | tf_op jit(solution)/shard_map/new_state/pallas_call | solution.py:304
  106.8 3.9 %all-to-all-done.3 = bf16[64,8,512]{2,1,0:T(8,128)(2,1)S(1)} async-done(((bf16[64,8,512]{2,1,0:T(8,128)(2,1)}), bf16[64,8,512]{2,1,0:T(8,128)(2,1)S(1)}, u32[]{:S(2)}, u32[]{:S(2)}) %all-to-all-start.3) | async-done | bytes 524320 | tf_op jit(solution)/shard_map/all_to_all | solution.py:344
  (40 shorter events, 3.6 us)
Async XLA Ops:
  0.6 87.8 %collective-permute-start.7 = (bf16[2048,512]{1,0:T(8,128)(2,1)}, bf16[2048,512]{1,0:T(8,128)(2,1)S(1)}, u32[]{:S(2)}, u32[]{:S(2)}) collective-permute-start(bf16[2048,512]{1,0:T(8,128)(2,1)} %g0.1), channel_id=1, source_target_pairs={{0,1},{1,0},{2,3},{3,2},{4,5},{5,4},{6,7},{7,6},{8,9},{9,8},{10,11... | collective-permute-start | bytes 6291464 | tf_op jit(solution)/shard_map/ppermute | solution.py:340
  0.7 87.7 %collective-permute-start.8 = (bf16[2048,512]{1,0:T(8,128)(2,1)}, bf16[2048,512]{1,0:T(8,128)(2,1)}, u32[]{:S(2)}, u32[]{:S(2)}) collective-permute-start(bf16[2048,512]{1,0:T(8,128)(2,1)} %u0.1), channel_id=1, source_target_pairs={{0,1},{1,0},{2,3},{3,2},{4,5},{5,4},{6,7},{7,6},{8,9},{9,8},{10,11... | collective-permute-start | bytes 6291464 | tf_op jit(solution)/shard_map/ppermute | solution.py:340
  1.2 87.2 %collective-permute-start.9 = (bf16[512,2048]{1,0:T(8,128)(2,1)}, bf16[512,2048]{1,0:T(8,128)(2,1)}, u32[]{:S(2)}, u32[]{:S(2)}) collective-permute-start(bf16[512,2048]{1,0:T(8,128)(2,1)} %d0.1), channel_id=1, source_target_pairs={{0,1},{1,0},{2,3},{3,2},{4,5},{5,4},{6,7},{7,6},{8,9},{9,8},{10,11... | collective-permute-start | bytes 6291464 | tf_op jit(solution)/shard_map/ppermute | solution.py:340
  3.0 9.9 %collective-permute-start = (bf16[64,2048]{1,0:T(8,128)(2,1)S(1)}, bf16[64,2048]{1,0:T(8,128)(2,1)S(1)}, u32[]{:S(2)}, u32[]{:S(2)}) collective-permute-start(bf16[64,2048]{1,0:T(8,128)(2,1)S(1)} %get-tuple-element.16.o0), channel_id=1, source_target_pairs={{0,2},{2,4},{4,6},{6,0},{1,3},{3,5},{5,7},{7,1},{8,10},{10,12},{12... | collective-permute-start | bytes 786440 | tf_op jit(solution)/shard_map/ppermute | solution.py:388
  4.6 14.9 %collective-permute-start.1 = (bf16[64,2048]{1,0:T(8,128)(2,1)S(1)}, bf16[64,2048]{1,0:T(8,128)(2,1)S(1)}, u32[]{:S(2)}, u32[]{:S(2)}) collective-permute-start(bf16[64,2048]{1,0:T(8,128)(2,1)S(1)} %get-tuple-element.16.o0), channel_id=1, source_target_pairs={{0,4},{2,6},{4,0},{6,2},{1,5},{3,7},{5,1},{7,3},{8,12},{10,14},{12... | collective-permute-start | bytes 786440 | tf_op jit(solution)/shard_map/ppermute | solution.py:388
  12.9 7.8 %collective-permute-start.2 = (bf16[64,2048]{1,0:T(8,128)(2,1)S(1)}, bf16[64,2048]{1,0:T(8,128)(2,1)S(1)}, u32[]{:S(2)}, u32[]{:S(2)}) collective-permute-start(bf16[64,2048]{1,0:T(8,128)(2,1)S(1)} %get-tuple-element.16.o0), channel_id=1, source_target_pairs={{0,6},{2,0},{4,2},{6,4},{1,7},{3,1},{5,3},{7,5},{8,14},{10,8},{12,... | collective-permute-start | bytes 786440 | tf_op jit(solution)/shard_map/ppermute | solution.py:388
  19.6 9.9 %collective-permute-start.3 = (bf16[64,2048]{1,0:T(8,128)(2,1)S(1)}, bf16[64,2048]{1,0:T(8,128)(2,1)}, u32[]{:S(2)}, u32[]{:S(2)}) collective-permute-start(bf16[64,2048]{1,0:T(8,128)(2,1)S(1)} %get-tuple-element.16.o0), channel_id=1, source_target_pairs={{0,1},{1,0},{2,3},{3,2},{4,5},{5,4},{6,7},{7,6},{8,9},{9,8},{10,11... | collective-permute-start | bytes 786440 | tf_op jit(solution)/shard_map/ppermute | solution.py:340
  21.3 8.5 %collective-permute-start.4 = (bf16[64,2048]{1,0:T(8,128)(2,1)S(1)}, bf16[64,2048]{1,0:T(8,128)(2,1)}, u32[]{:S(2)}, u32[]{:S(2)}) collective-permute-start(bf16[64,2048]{1,0:T(8,128)(2,1)S(1)} %collective-permute-done.o1), channel_id=1, source_target_pairs={{0,1},{1,0},{2,3},{3,2},{4,5},{5,4},{6,7},{7,6},{8,9},{9,8},{10,11... | collective-permute-start | bytes 786440 | tf_op jit(solution)/shard_map/ppermute | solution.py:340
  21.3 20.4 %all-to-all-start = ((bf16[16,8,2048]{2,1,0:T(8,128)(2,1)}), bf16[16,8,2048]{2,1,0:T(8,128)(2,1)S(1)}, u32[]{:S(2)}, u32[]{:S(2)}) async-start(bf16[16,8,2048]{2,1,0:T(8,128)(2,1)} %get-tuple-element.15), calls=%async_computation | async-start | bytes 1048576 | tf_op jit(solution)/shard_map/all_to_all | solution.py:344
  29.5 12.2 %collective-permute-start.5 = (bf16[64,2048]{1,0:T(8,128)(2,1)S(1)}, bf16[64,2048]{1,0:T(8,128)(2,1)}, u32[]{:S(2)}, u32[]{:S(2)}) collective-permute-start(bf16[64,2048]{1,0:T(8,128)(2,1)S(1)} %collective-permute-done.1.o2), channel_id=1, source_target_pairs={{0,1},{1,0},{2,3},{3,2},{4,5},{5,4},{6,7},{7,6},{8,9},{9,8},{10,11... | collective-permute-start | bytes 786440 | tf_op jit(solution)/shard_map/ppermute | solution.py:340
  29.8 11.9 %collective-permute-start.6 = (bf16[64,2048]{1,0:T(8,128)(2,1)}, bf16[64,2048]{1,0:T(8,128)(2,1)}, u32[]{:S(2)}, u32[]{:S(2)}) collective-permute-start(bf16[64,2048]{1,0:T(8,128)(2,1)} %copy-done.8), channel_id=1, source_target_pairs={{0,1},{1,0},{2,3},{3,2},{4,5},{5,4},{6,7},{7,6},{8,9},{9,8},{10,11... | collective-permute-start | bytes 786440 | tf_op jit(solution)/shard_map/ppermute | solution.py:340
  42.7 20.0 %copy-start.7 = (bf16[8,2048]{1,0:T(8,128)(2,1)S(1)}, bf16[8,2048]{1,0:T(8,128)(2,1)}, u32[]{:S(2)}) copy-start(bf16[8,2048]{1,0:T(8,128)(2,1)} %x_ref.3) | copy-start | bytes 98308
  42.7 20.0 %copy-start.11 = (f32[2048]{0:T(1024)S(1)}, f32[2048]{0:T(1024)}, u32[]{:S(2)}) copy-start(f32[2048]{0:T(1024)} %param.33) | copy-start | bytes 24580
  42.7 20.0 %copy-start.12 = (f32[2048]{0:T(1024)S(1)}, f32[2048]{0:T(1024)}, u32[]{:S(2)}) copy-start(f32[2048]{0:T(1024)} %param.35) | copy-start | bytes 24580
  42.7 20.0 %copy-start.14 = (f32[128]{0:T(128)S(1)}, f32[128]{0:T(128)}, u32[]{:S(2)}) copy-start(f32[128]{0:T(128)} %param.31) | copy-start | bytes 1540
  47.1 2.0 %copy-start = (bf16[8,16,128,128]{3,2,1,0:T(8,128)(2,1)}, bf16[8,16,128,128]{3,2,1,0:T(8,128)(2,1)S(1)}, u32[]{:S(2)}) copy-start(bf16[8,16,128,128]{3,2,1,0:T(8,128)(2,1)S(1)} %get-tuple-element.22.state_ref) | copy-start | bytes 12582916
  51.2 11.5 %all-to-all-start.1 = ((bf16[16,8,512]{2,1,0:T(8,128)(2,1)}), bf16[16,8,512]{2,1,0:T(8,128)(2,1)S(1)}, u32[]{:S(2)}, u32[]{:S(2)}) async-start(bf16[16,8,512]{2,1,0:T(8,128)(2,1)} %bitcast.25), calls=%async_computation.1 | async-start | bytes 262144 | tf_op jit(solution)/shard_map/all_to_all | solution.py:344
  62.7 2.2 %copy-start.1 = (bf16[8,16,128,128]{3,2,1,0:T(8,128)(2,1)S(1)}, bf16[8,16,128,128]{3,2,1,0:T(8,128)(2,1)}, u32[]{:S(2)}) copy-start(bf16[8,16,128,128]{3,2,1,0:T(8,128)(2,1)} %copy-done) | copy-start | bytes 12582916
  64.9 1.6 %copy-start.6 = (bf16[512,2048]{1,0:T(8,128)(2,1)S(1)}, bf16[512,2048]{1,0:T(8,128)(2,1)}, u32[]{:S(2)}) copy-start(bf16[512,2048]{1,0:T(8,128)(2,1)} %copy-done.5) | copy-start | bytes 6291460
  66.5 22.0 %copy-start.2 = (bf16[2048,512]{1,0:T(8,128)(2,1)S(1)}, bf16[2048,512]{1,0:T(8,128)(2,1)}, u32[]{:S(2)}) copy-start(bf16[2048,512]{1,0:T(8,128)(2,1)} %g0.1) | copy-start | bytes 6291460
  66.5 22.0 %copy-start.3 = (bf16[2048,512]{1,0:T(8,128)(2,1)S(1)}, bf16[2048,512]{1,0:T(8,128)(2,1)}, u32[]{:S(2)}) copy-start(bf16[2048,512]{1,0:T(8,128)(2,1)} %u0.1) | copy-start | bytes 6291460
  66.5 22.0 %copy-start.4 = (bf16[512,2048]{1,0:T(8,128)(2,1)S(1)}, bf16[512,2048]{1,0:T(8,128)(2,1)}, u32[]{:S(2)}) copy-start(bf16[512,2048]{1,0:T(8,128)(2,1)} %d0.1) | copy-start | bytes 6291460
  94.0 16.7 %all-to-all-start.3 = ((bf16[64,8,512]{2,1,0:T(8,128)(2,1)}), bf16[64,8,512]{2,1,0:T(8,128)(2,1)S(1)}, u32[]{:S(2)}, u32[]{:S(2)}) async-start(bf16[64,8,512]{2,1,0:T(8,128)(2,1)} %bitcast.18), calls=%async_computation.3 | async-start | bytes 1048576 | tf_op jit(solution)/shard_map/all_to_all | solution.py:344
  98.7 12.0 %copy-start.13 = (f32[2048]{0:T(1024)S(1)}, f32[2048]{0:T(1024)}, u32[]{:S(2)}) copy-start(f32[2048]{0:T(1024)} %param.41) | copy-start | bytes 24580
  (4 other events, 3.7 us)

commit v4 on v3

--- a/solution.py
+++ b/solution.py
@@ -20,9 +20,9 @@
 RUN = D // QUART
 LINES = CHIPS * CAP * QUART
 ROWS = CHIPS * CAP
-PARTS = 4
+PARTS = 7
 GROUP = 8
-EARLY = 512
+EARLY = 256
 LATER = D - EARLY
 
 
@@ -179,6 +179,7 @@
     w_near_ref,
     weights_ref,
     near_ref,
+    ready_ref,
     sems,
 ):
     fetch = pltpu.make_async_copy(gain_ref, near_ref, sems.at[SEQ + 1])
@@ -201,7 +202,14 @@
     scaled = rms_scale(rows_ref[...].astype(F32))
     fetch.wait()
     normed = (scaled * near_ref[...]).astype(BF16)
-    out_ref[...] = nt(normed, weights_ref[...]).astype(BF16)
+    ready_ref[...] = normed
+
+    def one_kind(kind, carry):
+        lines = pl.ds(pl.multiple_of(kind * 2 * HD, 2 * HD), 2 * HD)
+        out_ref[:, lines] = nt(ready_ref[...], weights_ref[lines, :]).astype(BF16)
+        return carry
+
+    lax.fori_loop(0, 2, one_kind, 0)
     for copy in later:
         copy.wait()
 
@@ -403,6 +411,7 @@
         scratch=[
             pltpu.VMEM((4 * HD, D), BF16),
             pltpu.VMEM((1, D), F32),
+            pltpu.VMEM((ZY * SEQ, D), BF16),
             pltpu.SemaphoreType.DMA((SEQ + 2,)),
         ],
         specs=[vmem, far, far, far] + [vmem] * 8,

time: 112 us -> 112 us (level)
  no operation moved by 1% of the time
where the time goes in v4:
time: 112 us; the launch traced here: 111 us
  waiting for transfers between devices  32.7 us (29%)
  Pallas kernels  26 us (23%)
  starting transfers between devices  24.3 us (22%)
  blocking collectives  18.2 us (16%)
  local copies, waits for them, and re-layouts  8.82 us (8%)
    all_to_all x3, waiting for transfers between devices, exchange(): return lax.all_to_all(values, axes, 0, 0, tiled=True)  21.7 us
    all_to_all x1, blocking collectives, exchange(): return lax.all_to_all(values, axes, 0, 0, tiled=True)  18.2 us
    all_to_all x3, starting transfers between devices, exchange(): return lax.all_to_all(values, axes, 0, 0, tiled=True)  16.4 us
    ppermute x3, waiting for transfers between devices, shards(): lax.ppermute(own, 'x', [(i, (i + shift) % 4) for i in range(4)])  11.1 us
    unnamed x30, local copies, waits for them, and re-layouts  8.82 us
    pallas_call x1, Pallas kernels, state_call(): pl.pallas_call(state_body, grid=(H // HEADS,), in_specs=[small, small, sm...  8.01 us
    ppermute x3, starting transfers between devices, shards(): lax.ppermute(own, 'x', [(i, (i + shift) % 4) for i in range(4)])  6.62 us
    pallas_call x1, Pallas kernels, shards(): call(expert_body, shape((LINES, RUN), BF16), 16)  5.54 us
  transfers between devices with their start and end apart: 13, of which 6 were waited for; matrix products, arithmetic and copies ran while one was open for 0% of the time, Pallas kernels for 18%

profile of v4, /device:TPU:0, one launch (start us, length us, event | category | flops | bytes accessed | tf_op | source)
XLA Modules:
  0.0 110.8 jit_solution(13004375307109285945)
XLA Ops:
  1.3 1.6 %shard_map.212 = (bf16[16,8,2048]{2,1,0:T(8,128)(2,1)}, bf16[64,2048]{1,0:T(8,128)(2,1)S(1)}) custom-call(bf16[8,2048]{1,0:T(8,128)(2,1)} %x_ref.3, bf16[16,2048]{1,0:T(8,128)(2,1)} %bitcast.30, bf16[16,2048]{1,0:T(8,128)(2,1)} %bitcast.31, bf16[16,2048]{1,0:T(8,128)(2,1)} %bitcast.32, bf16[16,2048]{1,0:T(8,128)(2,1)} %bitcast.33), custom_call_target="tpu_custom_call" | custom-call | tf_op jit(solution)/shard_map/pallas_call | solution.py:382
  3.0 1.7 %collective-permute-start = (bf16[64,2048]{1,0:T(8,128)(2,1)S(1)}, bf16[64,2048]{1,0:T(8,128)(2,1)S(1)}, u32[]{:S(2)}, u32[]{:S(2)}) collective-permute-start(bf16[64,2048]{1,0:T(8,128)(2,1)S(1)} %get-tuple-element.16.o0), channel_id=1, source_target_pairs={{0,2},{2,4},{4,6},{6,0},{1,3},{3,5},{5,7},{7,1},{8,10},{10,12},{12... | collective-permute-start | bytes 786440 | tf_op jit(solution)/shard_map/ppermute | solution.py:396
  4.6 2.7 %collective-permute-start.1 = (bf16[64,2048]{1,0:T(8,128)(2,1)S(1)}, bf16[64,2048]{1,0:T(8,128)(2,1)S(1)}, u32[]{:S(2)}, u32[]{:S(2)}) collective-permute-start(bf16[64,2048]{1,0:T(8,128)(2,1)S(1)} %get-tuple-element.16.o0), channel_id=1, source_target_pairs={{0,4},{2,6},{4,0},{6,2},{1,5},{3,7},{5,1},{7,3},{8,12},{10,14},{12... | collective-permute-start | bytes 786440 | tf_op jit(solution)/shard_map/ppermute | solution.py:396
  7.4 5.5 %collective-permute-done.o1 = bf16[64,2048]{1,0:T(8,128)(2,1)S(1)} collective-permute-done((bf16[64,2048]{1,0:T(8,128)(2,1)S(1)}, bf16[64,2048]{1,0:T(8,128)(2,1)S(1)}, u32[]{:S(2)}, u32[]{:S(2)}) %collective-permute-start) | collective-permute-done | bytes 262176 | tf_op jit(solution)/shard_map/ppermute | solution.py:396
  12.9 2.2 %collective-permute-start.2 = (bf16[64,2048]{1,0:T(8,128)(2,1)S(1)}, bf16[64,2048]{1,0:T(8,128)(2,1)S(1)}, u32[]{:S(2)}, u32[]{:S(2)}) collective-permute-start(bf16[64,2048]{1,0:T(8,128)(2,1)S(1)} %get-tuple-element.16.o0), channel_id=1, source_target_pairs={{0,6},{2,0},{4,2},{6,4},{1,7},{3,1},{5,3},{7,5},{8,14},{10,8},{12,... | collective-permute-start | bytes 786440 | tf_op jit(solution)/shard_map/ppermute | solution.py:396
  15.1 4.5 %collective-permute-done.1.o2 = bf16[64,2048]{1,0:T(8,128)(2,1)S(1)} collective-permute-done((bf16[64,2048]{1,0:T(8,128)(2,1)S(1)}, bf16[64,2048]{1,0:T(8,128)(2,1)S(1)}, u32[]{:S(2)}, u32[]{:S(2)}) %collective-permute-start.1) | collective-permute-done | bytes 262176 | tf_op jit(solution)/shard_map/ppermute | solution.py:396
  19.6 1.0 collective-permute-done.2.o3
  21.3 8.2 %all-to-all-start = ((bf16[16,8,2048]{2,1,0:T(8,128)(2,1)}), bf16[16,8,2048]{2,1,0:T(8,128)(2,1)S(1)}, u32[]{:S(2)}, u32[]{:S(2)}) async-start(bf16[16,8,2048]{2,1,0:T(8,128)(2,1)} %get-tuple-element.15), calls=%async_computation | async-start | bytes 1048576 | tf_op jit(solution)/shard_map/all_to_all | solution.py:352
  30.1 11.6 %all-to-all-done = bf16[16,8,2048]{2,1,0:T(8,128)(2,1)S(1)} async-done(((bf16[16,8,2048]{2,1,0:T(8,128)(2,1)}), bf16[16,8,2048]{2,1,0:T(8,128)(2,1)S(1)}, u32[]{:S(2)}, u32[]{:S(2)}) %all-to-all-start) | async-done | bytes 524320 | tf_op jit(solution)/shard_map/all_to_all | solution.py:352
  41.7 0.9 copy-done.9
  42.7 4.1 %shard_map.213 = (bf16[128,512]{1,0:T(8,128)(2,1)S(1)}, bf16[8,16,128,128]{3,2,1,0:T(8,128)(2,1)S(1)}, bf16[256,2048]{1,0:T(8,128)(2,1)S(1)}) custom-call(bf16[128,2048]{1,0:T(8,128)(2,1)S(1)} %bitcast.21, f32[1,2048]{1,0:T(1,128)} %bitcast.36, bf16[8,16,128,128]{3,2,1,0:T(8,128)(2,1)} %state_ref.3, bf16[2048,2048]{1,0:T(8,128)(2,1)} %w_last_ref.1, ...), custom_call_target="tpu_custom_call" | custom-call | tf_op jit(solution)/shard_map/pallas_call | solution.py:403
  46.8 2.0 %copy-done = bf16[8,16,128,128]{3,2,1,0:T(8,128)(2,1)} copy-done((bf16[8,16,128,128]{3,2,1,0:T(8,128)(2,1)}, bf16[8,16,128,128]{3,2,1,0:T(8,128)(2,1)S(1)}, u32[]{:S(2)}) %copy-start) | copy-done | bytes 4194328
  48.8 1.0 copy-done.5
  50.5 3.5 %all-to-all-start.1 = ((bf16[16,8,512]{2,1,0:T(8,128)(2,1)}), bf16[16,8,512]{2,1,0:T(8,128)(2,1)S(1)}, u32[]{:S(2)}, u32[]{:S(2)}) async-start(bf16[16,8,512]{2,1,0:T(8,128)(2,1)} %bitcast.25), calls=%async_computation.1 | async-start | bytes 262144 | tf_op jit(solution)/shard_map/all_to_all | solution.py:352
  54.0 1.8 %shard_map.214 = (bf16[512,32]{1,0:T(8,128)(2,1)S(1)}, bf16[64,512]{1,0:T(8,128)(2,1)S(1)}, f32[16,8,128]{2,1,0:T(8,128)S(1)}, f32[16,8,128]{2,1,0:T(8,128)S(1)}) custom-call(s32[4,8]{1,0:T(4,128)} %bitcast.38, f32[4,8]{1,0:T(4,128)} %bitcast.39, bf16[8,2048]{1,0:T(8,128)(2,1)} %x_ref.3, f32[1,2048]{1,0:T(1,128)} %bitcast.37, bf16[16,2048]{1,0:T(8,128)(2,1)} %bitcast.34, ...), custom_call_target="tpu_custom_call" | custom-call | tf_op jit(solution)/shard_map/pallas_call | solution.py:437
  55.8 6.1 %all-to-all-done.1.joined_ref = bf16[16,8,512]{2,1,0:T(8,128)(2,1)S(1)} async-done(((bf16[16,8,512]{2,1,0:T(8,128)(2,1)}), bf16[16,8,512]{2,1,0:T(8,128)(2,1)S(1)}, u32[]{:S(2)}, u32[]{:S(2)}) %all-to-all-start.1) | async-done | bytes 131104 | tf_op jit(solution)/shard_map/all_to_all | solution.py:352
  62.0 2.2 %copy-done.1 = bf16[8,16,128,128]{3,2,1,0:T(8,128)(2,1)S(1)} copy-done((bf16[8,16,128,128]{3,2,1,0:T(8,128)(2,1)S(1)}, bf16[8,16,128,128]{3,2,1,0:T(8,128)(2,1)}, u32[]{:S(2)}) %copy-start.1) | copy-done | bytes 4194328
  64.2 1.2 %copy-done.6 = bf16[256,2048]{1,0:T(8,128)(2,1)S(1)} copy-done((bf16[256,2048]{1,0:T(8,128)(2,1)S(1)}, bf16[256,2048]{1,0:T(8,128)(2,1)}, u32[]{:S(2)}) %copy-start.6) | copy-done | bytes 1048600
  65.4 4.0 %shard_map.215 = (bf16[512,512]{1,0:T(8,128)(2,1)S(1)}, f32[8,2048]{1,0:T(8,128)S(1)}, f32[16,8,128]{2,1,0:T(8,128)S(1)}, f32[16,8,128]{2,1,0:T(8,128)S(1)}) custom-call(bf16[16,8,512]{2,1,0:T(8,128)(2,1)S(1)} %all-to-all-done.1.joined_ref, bf16[8,2048]{1,0:T(8,128)(2,1)S(1)} %copy-done.7, f32[16,8,128]{2,1,0:T(8,128)S(1)} %get-tuple-element.18.fade_ref, ...), custom_call_target="tpu_custom_call" | custom-call | tf_op jit(solution)/shard_map/pallas_call | solution.py:452
  69.4 18.2 %all_to_all.20 = bf16[64,8,512]{2,1,0:T(8,128)(2,1)S(1)} all-to-all(bf16[64,8,512]{2,1,0:T(8,128)(2,1)S(1)} %bitcast.24), channel_id=1, replica_groups=mesh['z'=4,'y'=4,'x'=4,'c'=2] {'z','y','x'}, dimensions={0} | all-to-all | bytes 1048576 | tf_op jit(solution)/shard_map/all_to_all | solution.py:352
  87.6 5.5 %shard_map.216 = bf16[512,512]{1,0:T(8,128)(2,1)} custom-call(bf16[512,512]{1,0:T(8,128)(2,1)S(1)} %bitcast.23, bf16[2048,512]{1,0:T(8,128)(2,1)S(1)} %copy-done.2, bf16[2048,512]{1,0:T(8,128)(2,1)S(1)} %collective-permute-done.7.g1, bf16[2048,512]{1,0:T(8,128)(2,1)S(1)} %copy-done.3, bf16[2048,512]{1,0:T(8,128)(2,1)} %collective-permute-done.8.u1, ...), custom_call_target="tpu_custom_call" | custom-call | tf_op jit(solution)/shard_map/pallas_call | solution.py:477
  93.2 4.7 %all-to-all-start.3 = ((bf16[64,8,512]{2,1,0:T(8,128)(2,1)}), bf16[64,8,512]{2,1,0:T(8,128)(2,1)S(1)}, u32[]{:S(2)}, u32[]{:S(2)}) async-start(bf16[64,8,512]{2,1,0:T(8,128)(2,1)} %bitcast.18), calls=%async_computation.3 | async-start | bytes 1048576 | tf_op jit(solution)/shard_map/all_to_all | solution.py:352
  97.9 8.0 %new_state.1 = bf16[8,16,128,128]{3,2,1,0:T(8,128)(2,1)} custom-call(f32[16,8,128]{2,1,0:T(8,128)S(1)} %get-tuple-element.26.keys_ref, f32[16,8,128]{2,1,0:T(8,128)S(1)} %get-tuple-element.27.change_ref, f32[16,8,128]{2,1,0:T(8,128)S(1)} %get-tuple-element.18.fade_ref, bf16[8,16,128,128]{3,2,1,0:T(8,128)(2,1)} %state_ref.3), custom_call_target="tpu_custom_call" | custom-call | flops 40000000 | bytes 8388608 | tf_op jit(solution)/shard_map/new_state/pallas_call | solution.py:312
  105.9 3.9 %all-to-all-done.3 = bf16[64,8,512]{2,1,0:T(8,128)(2,1)S(1)} async-done(((bf16[64,8,512]{2,1,0:T(8,128)(2,1)}), bf16[64,8,512]{2,1,0:T(8,128)(2,1)S(1)}, u32[]{:S(2)}, u32[]{:S(2)}) %all-to-all-start.3) | async-done | bytes 524320 | tf_op jit(solution)/shard_map/all_to_all | solution.py:352
  (40 shorter events, 3.6 us)
Async XLA Ops:
  0.6 87.0 %collective-permute-start.7 = (bf16[2048,512]{1,0:T(8,128)(2,1)}, bf16[2048,512]{1,0:T(8,128)(2,1)S(1)}, u32[]{:S(2)}, u32[]{:S(2)}) collective-permute-start(bf16[2048,512]{1,0:T(8,128)(2,1)} %g0.1), channel_id=1, source_target_pairs={{0,1},{1,0},{2,3},{3,2},{4,5},{5,4},{6,7},{7,6},{8,9},{9,8},{10,11... | collective-permute-start | bytes 6291464 | tf_op jit(solution)/shard_map/ppermute | solution.py:348
  0.7 86.9 %collective-permute-start.8 = (bf16[2048,512]{1,0:T(8,128)(2,1)}, bf16[2048,512]{1,0:T(8,128)(2,1)}, u32[]{:S(2)}, u32[]{:S(2)}) collective-permute-start(bf16[2048,512]{1,0:T(8,128)(2,1)} %u0.1), channel_id=1, source_target_pairs={{0,1},{1,0},{2,3},{3,2},{4,5},{5,4},{6,7},{7,6},{8,9},{9,8},{10,11... | collective-permute-start | bytes 6291464 | tf_op jit(solution)/shard_map/ppermute | solution.py:348
  1.2 86.4 %collective-permute-start.9 = (bf16[512,2048]{1,0:T(8,128)(2,1)}, bf16[512,2048]{1,0:T(8,128)(2,1)}, u32[]{:S(2)}, u32[]{:S(2)}) collective-permute-start(bf16[512,2048]{1,0:T(8,128)(2,1)} %d0.1), channel_id=1, source_target_pairs={{0,1},{1,0},{2,3},{3,2},{4,5},{5,4},{6,7},{7,6},{8,9},{9,8},{10,11... | collective-permute-start | bytes 6291464 | tf_op jit(solution)/shard_map/ppermute | solution.py:348
  3.0 9.9 %collective-permute-start = (bf16[64,2048]{1,0:T(8,128)(2,1)S(1)}, bf16[64,2048]{1,0:T(8,128)(2,1)S(1)}, u32[]{:S(2)}, u32[]{:S(2)}) collective-permute-start(bf16[64,2048]{1,0:T(8,128)(2,1)S(1)} %get-tuple-element.16.o0), channel_id=1, source_target_pairs={{0,2},{2,4},{4,6},{6,0},{1,3},{3,5},{5,7},{7,1},{8,10},{10,12},{12... | collective-permute-start | bytes 786440 | tf_op jit(solution)/shard_map/ppermute | solution.py:396
  4.6 14.9 %collective-permute-start.1 = (bf16[64,2048]{1,0:T(8,128)(2,1)S(1)}, bf16[64,2048]{1,0:T(8,128)(2,1)S(1)}, u32[]{:S(2)}, u32[]{:S(2)}) collective-permute-start(bf16[64,2048]{1,0:T(8,128)(2,1)S(1)} %get-tuple-element.16.o0), channel_id=1, source_target_pairs={{0,4},{2,6},{4,0},{6,2},{1,5},{3,7},{5,1},{7,3},{8,12},{10,14},{12... | collective-permute-start | bytes 786440 | tf_op jit(solution)/shard_map/ppermute | solution.py:396
  12.9 7.8 %collective-permute-start.2 = (bf16[64,2048]{1,0:T(8,128)(2,1)S(1)}, bf16[64,2048]{1,0:T(8,128)(2,1)S(1)}, u32[]{:S(2)}, u32[]{:S(2)}) collective-permute-start(bf16[64,2048]{1,0:T(8,128)(2,1)S(1)} %get-tuple-element.16.o0), channel_id=1, source_target_pairs={{0,6},{2,0},{4,2},{6,4},{1,7},{3,1},{5,3},{7,5},{8,14},{10,8},{12,... | collective-permute-start | bytes 786440 | tf_op jit(solution)/shard_map/ppermute | solution.py:396
  19.6 9.9 %collective-permute-start.3 = (bf16[64,2048]{1,0:T(8,128)(2,1)S(1)}, bf16[64,2048]{1,0:T(8,128)(2,1)}, u32[]{:S(2)}, u32[]{:S(2)}) collective-permute-start(bf16[64,2048]{1,0:T(8,128)(2,1)S(1)} %get-tuple-element.16.o0), channel_id=1, source_target_pairs={{0,1},{1,0},{2,3},{3,2},{4,5},{5,4},{6,7},{7,6},{8,9},{9,8},{10,11... | collective-permute-start | bytes 786440 | tf_op jit(solution)/shard_map/ppermute | solution.py:348
  21.3 8.5 %collective-permute-start.4 = (bf16[64,2048]{1,0:T(8,128)(2,1)S(1)}, bf16[64,2048]{1,0:T(8,128)(2,1)}, u32[]{:S(2)}, u32[]{:S(2)}) collective-permute-start(bf16[64,2048]{1,0:T(8,128)(2,1)S(1)} %collective-permute-done.o1), channel_id=1, source_target_pairs={{0,1},{1,0},{2,3},{3,2},{4,5},{5,4},{6,7},{7,6},{8,9},{9,8},{10,11... | collective-permute-start | bytes 786440 | tf_op jit(solution)/shard_map/ppermute | solution.py:348
  21.3 20.4 %all-to-all-start = ((bf16[16,8,2048]{2,1,0:T(8,128)(2,1)}), bf16[16,8,2048]{2,1,0:T(8,128)(2,1)S(1)}, u32[]{:S(2)}, u32[]{:S(2)}) async-start(bf16[16,8,2048]{2,1,0:T(8,128)(2,1)} %get-tuple-element.15), calls=%async_computation | async-start | bytes 1048576 | tf_op jit(solution)/shard_map/all_to_all | solution.py:352
  29.5 12.2 %collective-permute-start.5 = (bf16[64,2048]{1,0:T(8,128)(2,1)S(1)}, bf16[64,2048]{1,0:T(8,128)(2,1)}, u32[]{:S(2)}, u32[]{:S(2)}) collective-permute-start(bf16[64,2048]{1,0:T(8,128)(2,1)S(1)} %collective-permute-done.1.o2), channel_id=1, source_target_pairs={{0,1},{1,0},{2,3},{3,2},{4,5},{5,4},{6,7},{7,6},{8,9},{9,8},{10,11... | collective-permute-start | bytes 786440 | tf_op jit(solution)/shard_map/ppermute | solution.py:348
  29.8 11.9 %collective-permute-start.6 = (bf16[64,2048]{1,0:T(8,128)(2,1)}, bf16[64,2048]{1,0:T(8,128)(2,1)}, u32[]{:S(2)}, u32[]{:S(2)}) collective-permute-start(bf16[64,2048]{1,0:T(8,128)(2,1)} %copy-done.8), channel_id=1, source_target_pairs={{0,1},{1,0},{2,3},{3,2},{4,5},{5,4},{6,7},{7,6},{8,9},{9,8},{10,11... | collective-permute-start | bytes 786440 | tf_op jit(solution)/shard_map/ppermute | solution.py:348
  42.7 19.3 %copy-start.7 = (bf16[8,2048]{1,0:T(8,128)(2,1)S(1)}, bf16[8,2048]{1,0:T(8,128)(2,1)}, u32[]{:S(2)}) copy-start(bf16[8,2048]{1,0:T(8,128)(2,1)} %x_ref.3) | copy-start | bytes 98308
  42.7 19.3 %copy-start.11 = (f32[2048]{0:T(1024)S(1)}, f32[2048]{0:T(1024)}, u32[]{:S(2)}) copy-start(f32[2048]{0:T(1024)} %param.33) | copy-start | bytes 24580
  42.7 19.3 %copy-start.12 = (f32[2048]{0:T(1024)S(1)}, f32[2048]{0:T(1024)}, u32[]{:S(2)}) copy-start(f32[2048]{0:T(1024)} %param.35) | copy-start | bytes 24580
  42.7 19.3 %copy-start.14 = (f32[128]{0:T(128)S(1)}, f32[128]{0:T(128)}, u32[]{:S(2)}) copy-start(f32[128]{0:T(128)} %param.31) | copy-start | bytes 1540
  46.8 2.0 %copy-start = (bf16[8,16,128,128]{3,2,1,0:T(8,128)(2,1)}, bf16[8,16,128,128]{3,2,1,0:T(8,128)(2,1)S(1)}, u32[]{:S(2)}) copy-start(bf16[8,16,128,128]{3,2,1,0:T(8,128)(2,1)S(1)} %get-tuple-element.22.state_ref) | copy-start | bytes 12582916
  50.5 11.5 %all-to-all-start.1 = ((bf16[16,8,512]{2,1,0:T(8,128)(2,1)}), bf16[16,8,512]{2,1,0:T(8,128)(2,1)S(1)}, u32[]{:S(2)}, u32[]{:S(2)}) async-start(bf16[16,8,512]{2,1,0:T(8,128)(2,1)} %bitcast.25), calls=%async_computation.1 | async-start | bytes 262144 | tf_op jit(solution)/shard_map/all_to_all | solution.py:352
  62.0 2.2 %copy-start.1 = (bf16[8,16,128,128]{3,2,1,0:T(8,128)(2,1)S(1)}, bf16[8,16,128,128]{3,2,1,0:T(8,128)(2,1)}, u32[]{:S(2)}) copy-start(bf16[8,16,128,128]{3,2,1,0:T(8,128)(2,1)} %copy-done) | copy-start | bytes 12582916
  64.2 1.2 %copy-start.6 = (bf16[256,2048]{1,0:T(8,128)(2,1)S(1)}, bf16[256,2048]{1,0:T(8,128)(2,1)}, u32[]{:S(2)}) copy-start(bf16[256,2048]{1,0:T(8,128)(2,1)} %copy-done.5) | copy-start | bytes 3145732
  65.4 22.2 %copy-start.2 = (bf16[2048,512]{1,0:T(8,128)(2,1)S(1)}, bf16[2048,512]{1,0:T(8,128)(2,1)}, u32[]{:S(2)}) copy-start(bf16[2048,512]{1,0:T(8,128)(2,1)} %g0.1) | copy-start | bytes 6291460
  65.4 22.2 %copy-start.3 = (bf16[2048,512]{1,0:T(8,128)(2,1)S(1)}, bf16[2048,512]{1,0:T(8,128)(2,1)}, u32[]{:S(2)}) copy-start(bf16[2048,512]{1,0:T(8,128)(2,1)} %u0.1) | copy-start | bytes 6291460
  65.4 22.2 %copy-start.4 = (bf16[512,2048]{1,0:T(8,128)(2,1)S(1)}, bf16[512,2048]{1,0:T(8,128)(2,1)}, u32[]{:S(2)}) copy-start(bf16[512,2048]{1,0:T(8,128)(2,1)} %d0.1) | copy-start | bytes 6291460
  93.2 16.7 %all-to-all-start.3 = ((bf16[64,8,512]{2,1,0:T(8,128)(2,1)}), bf16[64,8,512]{2,1,0:T(8,128)(2,1)S(1)}, u32[]{:S(2)}, u32[]{:S(2)}) async-start(bf16[64,8,512]{2,1,0:T(8,128)(2,1)} %bitcast.18), calls=%async_computation.3 | async-start | bytes 1048576 | tf_op jit(solution)/shard_map/all_to_all | solution.py:352
  97.9 12.0 %copy-start.13 = (f32[2048]{0:T(1024)S(1)}, f32[2048]{0:T(1024)}, u32[]{:S(2)}) copy-start(f32[2048]{0:T(1024)} %param.41) | copy-start | bytes 24580
  (4 other events, 3.4 us)
